TPU v7x, 256 devices: a whole 4x4x8 slice. The times are simulated.
256 devices in a mesh: ep: 64 (over z, y, core), tp: 4 (over x).
Axes of the slice: x: 4, y: 4, z: 8, core: 2. Of those that a mesh axis runs over, the one named last changes fastest.
Arguments:
- tokens_a: bfloat16 [8192, 2048], P('ep'), may hold values from -30 to 30
- attn_gain: float32 [2048], replicated, may hold values from 0.1 to 1.9
- w_query: bfloat16 [2048, 2048], P(None, 'tp'), may hold values from -2 to 2
- w_query_rot: bfloat16 [2048, 1024], P(None, 'tp'), may hold values from -0.125 to 0.125
- w_latent: bfloat16 [2048, 512], replicated, may hold values from -2 to 2
- w_key_rot: bfloat16 [2048, 32], replicated, may hold values from -0.125 to 0.125
- latent_gain: float32 [512], replicated, may hold values from 0.1 to 1.9
- w_key_up: bfloat16 [512, 2048], P(None, 'tp'), may hold values from -2 to 2
- w_value_up: bfloat16 [512, 2048], P(None, 'tp'), may hold values from -0.25 to 0.25
- w_output: bfloat16 [2048, 2048], P('tp'), may hold values from -0.125 to 0.125
- tokens_b: bfloat16 [16384, 2048], P('ep'), may hold values from -6 to 6
- ffn_gain: float32 [2048], replicated, may hold values from 0.1 to 1.9
- expert_ids: int32 [16384, 2], P('ep'), may hold values from 0 to 63, all different within a row; in each aligned block of 256 rows (0 to 255, 256 to 511, ...) at most 16 rows name the same one
- expert_weights: float32 [16384, 2], P('ep'), may hold values from 0.1 to 1
- w_gate: bfloat16 [64, 2048, 1024], P('ep', None, 'tp'), may hold values from -0.125 to 0.125
- w_up: bfloat16 [64, 2048, 1024], P('ep', None, 'tp'), may hold values from -0.125 to 0.125
- w_down: bfloat16 [64, 1024, 2048], P('ep', 'tp'), may hold values from -0.1875 to 0.1875
Outputs:
- mixed_a: bfloat16 [8192, 2048], P(('ep', 'tp'))
- mixed_b: bfloat16 [16384, 2048], P('ep', 'tp')
Inputs may be any that keep to these rules, and one draw needn't show every extreme that they name: `expert_ids`: each row names 2 different experts. In the 256 rows of one index of ep no expert is named more than 16 times, and in some such block one expert is named exactly 16 times.
All inputs are finite; a program needn't handle non-finite values.
Results may differ from a plain program's by a relative error of at most 0.012.
Values may be sent and summed in bfloat16 or wider, within the bound.
No kernel may reach another device: no remote copies, remote signals or barrier semaphores. Data moves between devices by JAX's collectives and lax.ppermute only.
A program may use at most 192 MiB of HBM per device.

v0:
```python
import jax
import jax.numpy as jnp
from jax import lax
from jax.sharding import PartitionSpec as P

NOPE = 64
ROPE = 32
VD = 64


epsilon = 1e-06
rope_base = 10000.0


def normalize(matrix, gain):
    floats = matrix.astype(jnp.float32)
    scaled = floats * lax.rsqrt(jnp.mean(floats * floats, axis=-1, keepdims=True) + epsilon)
    return scaled * gain


def rotate(vectors, positions):
    rot_width = vectors.shape[-1]
    half_width = rot_width // 2
    inverse = rope_base ** (-(jnp.arange(half_width, dtype=jnp.float32) * 2.0) / rot_width)
    angles = positions.astype(jnp.float32)[:, None] * inverse[None, :]
    cosine = jnp.cos(angles)[:, None, :]
    sine_part = jnp.sin(angles)[:, None, :]
    first_half = vectors[..., :half_width]
    second_half = vectors[..., half_width:]
    return jnp.concatenate(
        [
            first_half * cosine - second_half * sine_part,
            first_half * sine_part + second_half * cosine,
        ],
        axis=-1,
    )


def attention_half(
    tokens_a,
    attn_gain,
    w_query,
    w_query_rot,
    w_latent,
    w_key_rot,
    latent_gain,
    w_key_up,
    w_value_up,
    w_output,
):
    row_count = tokens_a.shape[0]
    head_count = w_query.shape[1] // NOPE
    offset = lax.axis_index("ep") * row_count
    positions = offset + jnp.arange(row_count, dtype=jnp.int32)
    normed = normalize(tokens_a, attn_gain).astype(jnp.bfloat16)
    query_plain = jnp.dot(normed, w_query, preferred_element_type=jnp.float32).astype(jnp.bfloat16)
    query_plain = query_plain.reshape(row_count, head_count, NOPE)
    turned = jnp.dot(normed, w_query_rot, preferred_element_type=jnp.float32).reshape(
        row_count, head_count, ROPE
    )
    query_rotated_rows = rotate(turned, positions).astype(jnp.bfloat16)
    latent = normalize(
        jnp.dot(normed, w_latent, preferred_element_type=jnp.float32), latent_gain
    ).astype(jnp.bfloat16)
    key_raw = jnp.dot(normed, w_key_rot, preferred_element_type=jnp.float32)[:, None, :]
    key_turned = rotate(key_raw, positions)[:, 0, :].astype(jnp.bfloat16)
    logit_scale = (NOPE + ROPE) ** (-0.5)
    key_plain = jnp.dot(latent, w_key_up, preferred_element_type=jnp.float32).astype(jnp.bfloat16)
    values = jnp.dot(latent, w_value_up, preferred_element_type=jnp.float32).astype(jnp.bfloat16)
    update_key_plain = lax.all_gather(key_plain, "ep", axis=0, tiled=True)
    update_values = lax.all_gather(values, "ep", axis=0, tiled=True)
    key_count = update_key_plain.shape[0]
    blocks = key_count // row_count
    key_blocks = update_key_plain.reshape(blocks, row_count, head_count, NOPE)
    value_blocks = update_values.reshape(blocks, row_count, head_count, VD)
    rotated_key_blocks = lax.all_gather(key_turned, "ep", axis=0, tiled=True).reshape(
        blocks, row_count, ROPE
    )
    score_matrix = (
        jnp.einsum("yvz,wrvz->yvwr", query_plain, key_blocks, preferred_element_type=jnp.float32)
        + jnp.einsum(
            "yjx,inx->yjin",
            query_rotated_rows,
            rotated_key_blocks,
            preferred_element_type=jnp.float32,
        )
    ) * logit_scale
    key_pos = jnp.arange(key_count, dtype=jnp.int32).reshape(blocks, row_count)
    allowed = key_pos[None, None, :, :] <= positions[:, None, None, None]
    masked = jnp.where(allowed, score_matrix, -1e30)
    block_max = jnp.max(masked, axis=-1)
    probs = jnp.where(allowed, jnp.exp(masked - block_max[..., None]), 0.0)
    block_total = jnp.sum(probs, axis=-1)
    block_out = jnp.einsum(
        "qhbk,bkhd->qhbd",
        probs.astype(jnp.bfloat16),
        value_blocks,
        preferred_element_type=jnp.float32,
    )
    run_max = jnp.full((row_count, head_count), -1e30, jnp.float32)
    new_max = jnp.maximum(run_max, jnp.max(block_max, axis=-1))
    new_factor = jnp.exp(block_max - new_max[..., None])
    new_total = jnp.sum(new_factor * block_total, axis=-1)
    new_out = jnp.sum(new_factor[..., None] * block_out, axis=2)
    attended = (
        (new_out / new_total[..., None]).astype(jnp.bfloat16).reshape(row_count, head_count * VD)
    )
    return lax.psum_scatter(
        jnp.dot(attended, w_output, preferred_element_type=jnp.float32).astype(jnp.bfloat16),
        "tp",
        scatter_dimension=0,
        tiled=True,
    )


def expert_half(tokens_b, ffn_gain, expert_ids, expert_weights, w_gate, w_up, w_down):
    row_count = tokens_b.shape[0]
    top_count = expert_ids.shape[1]
    expert_count = w_gate.shape[0] * lax.axis_size("ep")
    capacity = 2 * row_count * top_count // expert_count
    normed = normalize(tokens_b, ffn_gain).astype(jnp.bfloat16)
    flat_ids = expert_ids.reshape(-1)
    pair_count = flat_ids.shape[0]
    onehot = (flat_ids[:, None] == jnp.arange(expert_count, dtype=jnp.int32)[None, :]).astype(
        jnp.int32
    )
    before = jnp.cumsum(onehot, axis=0) - onehot
    slot_index = jnp.sum(before * onehot, axis=1)
    target = flat_ids * capacity + slot_index
    source_row = (
        jnp.zeros((expert_count * capacity,), jnp.int32)
        .at[target]
        .set(jnp.arange(pair_count, dtype=jnp.int32) // top_count)
    )
    occupied = jnp.zeros((expert_count * capacity,), jnp.int32).at[target].set(1)
    outgoing = jnp.where(occupied[:, None] > 0, normed[source_row], jnp.zeros((), jnp.bfloat16))
    outgoing = outgoing.reshape(expert_count, capacity, normed.shape[1])
    gate_weight = w_gate[0]
    up_weight = w_up[0]
    down_weight = w_down[0]
    arrived = lax.all_to_all(outgoing, "ep", split_axis=0, concat_axis=0, tiled=True)
    flat_rows = arrived.reshape(-1, arrived.shape[-1])
    gate_part = jnp.dot(flat_rows, gate_weight, preferred_element_type=jnp.float32)
    up_part = jnp.dot(flat_rows, up_weight, preferred_element_type=jnp.float32)
    hidden_rows = (jax.nn.silu(gate_part) * up_part).astype(jnp.bfloat16)
    hidden = hidden_rows.reshape(arrived.shape[0], arrived.shape[1], gate_weight.shape[1])
    partial_value = jnp.dot(
        hidden.reshape(-1, hidden.shape[-1]), down_weight, preferred_element_type=jnp.float32
    )
    partial_value = partial_value.reshape(expert_count, capacity, down_weight.shape[1])
    summed = lax.psum_scatter(
        partial_value.astype(jnp.bfloat16), "tp", scatter_dimension=2, tiled=True
    )
    returned = lax.all_to_all(summed, "ep", split_axis=0, concat_axis=0, tiled=True)
    picked = returned.reshape(expert_count * capacity, -1)[target].astype(jnp.float32)
    picked = picked.reshape(row_count, top_count, -1)
    shares = expert_weights / jnp.sum(expert_weights, axis=1, keepdims=True)
    return jnp.sum(picked * shares[:, :, None], axis=1).astype(jnp.bfloat16)


def on_device(
    tokens_a,
    attn_gain,
    w_query,
    w_query_rot,
    w_latent,
    w_key_rot,
    latent_gain,
    w_key_up,
    w_value_up,
    w_output,
    tokens_b,
    ffn_gain,
    expert_ids,
    expert_weights,
    w_gate,
    w_up,
    w_down,
):
    mixed_a = attention_half(
        tokens_a,
        attn_gain,
        w_query,
        w_query_rot,
        w_latent,
        w_key_rot,
        latent_gain,
        w_key_up,
        w_value_up,
        w_output,
    )
    mixed_b = expert_half(tokens_b, ffn_gain, expert_ids, expert_weights, w_gate, w_up, w_down)
    return (mixed_a, mixed_b)


def solution(mesh):
    placed = (
        P("ep", None),
        P(),
        P(None, "tp"),
        P(None, "tp"),
        P(),
        P(),
        P(),
        P(None, "tp"),
        P(None, "tp"),
        P("tp", None),
        P("ep", None),
        P(),
        P("ep", None),
        P("ep", None),
        P("ep", None, "tp"),
        P("ep", None, "tp"),
        P("ep", "tp", None),
    )
    return jax.shard_map(
        on_device,
        mesh=mesh,
        in_specs=placed,
        out_specs=(P(("ep", "tp"), None), P("ep", "tp")),
        check_vma=False,
    )
```

profile of v0, /device:TPU:8, one launch (start us, length us, event | category | flops | bytes accessed | tf_op | source)
XLA Modules:
  0.0 389.7 jit_solution(2353448182346201327)
XLA Ops:
  9.4 2.4 multiply_reduce_fusion.2
  11.8 2.0 convolution_convert_fusion.4
  13.9 2.0 convolution_convert_fusion.2
  19.6 2.4 scatter_custom_fusion.1
  22.1 2.4 scatter_custom_fusion
  27.7 6.0 %gather_fusion = bf16[1024,2048]{1,0:T(8,128)(2,1)} fusion(bf16[256,2048]{1,0:T(8,128)(2,1)S(1)} %fusion.21, s32[1024]{0:T(1024)S(1)} %fusion.47), kind=kCustom, calls=%fused_computation | custom fusion | bytes 8392704 | tf_op jit(solution)/shard_map/gather | solution.py:136
  33.7 4.6 %broadcast_select_fusion = bf16[64,16,2048]{2,1,0:T(8,128)(2,1)} fusion(bf16[64,16,2048]{2,1,0:T(8,128)(2,1)} %bitcast.79, pred[64,16]{1,0:T(8,128)(4,1)S(1)} %broadcast_in_dim.76), kind=kLoop, calls=%fused_computation.19 | loop fusion | flops 2097152 | bytes 8389632 | tf_op jit(solution)/shard_map/jit(_where)/select_n | solution.py:136
  38.3 12.3 %all-to-all-start = ((bf16[64,16,2048]{2,1,0:T(8,128)(2,1)}), bf16[64,16,2048]{2,1,0:T(8,128)(2,1)}, u32[]{:S(2)}, u32[]{:S(2)}) async-start(bf16[64,16,2048]{2,1,0:T(8,128)(2,1)} %broadcast_select_fusion), calls=%async_computation.1 | async-start | bytes 8388608 | tf_op jit(solution)/shard_map/all_to_all | solution.py:141
  51.2 154.9 %all-gather = bf16[8192,1,32]{0,2,1:T(8,128)(2,1)S(1)} all-gather(bf16[128,1,32]{0,2,1:T(8,128)(2,1)S(1)} %pad_maximum_fusion), channel_id=2, replica_groups=mesh['ep'=64,'tp'=4] {'ep'}, dimensions={0}, use_global_device_ids=true | all-gather | bytes 532480 | tf_op jit(solution)/shard_map/all_gather | solution.py:76
  208.0 2.1 convolution_convert_fusion.3
  210.1 4.2 %fusion.28 = f32[1024,256]{1,0:T(8,128)S(1)} fusion(bf16[1024,2048]{1,0:T(8,128)(2,1)} %bitcast.15, bf16[1,2048,256]{2,1,0:T(8,128)(2,1)} %param.31), kind=kOutput, calls=%fused_computation.41 | convolution fusion | flops 1073741824 | bytes 6291456 | tf_op jit(solution)/shard_map/dot_general | solution.py:143
  214.4 3.9 fusion.22
  218.3 3.2 convolution_convert_fusion
  224.2 14.9 %fusion.30 = f32[128,8,64,128]{0,3,2,1:T(8,128)} fusion(bf16[64,128,32]{1,0,2:T(8,128)(2,1)} %bitcast.80, bf16[128,8,16]{0,2,1:T(8,128)(2,1)S(1)} %get-tuple-element.7, bf16[128,8,16]{0,2,1:T(8,128)(2,1)S(1)} %get-tuple-element.6), kind=kOutput, calls=%fused_computation.44 | convolution fusion | flops 537001984 | bytes 34144256 | tf_op jit(solution)/shard_map/yjx,inx->yjin/dot_general | solution.py:81
  239.1 21.2 %reshape.303 = bf16[64,128,8,64]{3,2,1,0:T(8,128)(2,1)} reshape(bf16[8192,512]{1,0:T(8,128)(2,1)} %all-gather.4.cloned.1.call-done) | data formatting | bytes 16777216 | tf_op jit(solution)/shard_map/reshape | solution.py:74
  260.4 21.2 %reshape.304 = bf16[64,128,8,64]{3,2,1,0:T(8,128)(2,1)} reshape(bf16[8192,512]{1,0:T(8,128)(2,1)} %all-gather.6.cloned.1.call-done) | data formatting | bytes 16777216 | tf_op jit(solution)/shard_map/reshape | solution.py:75
  281.6 27.4 %fusion.64 = (f32[128,8,64]{0,2,1:T(8,128)S(1)}, f32[128,8,64,128]{0,3,2,1:T(8,128)}) fusion(f32[128,8,64,128]{0,3,2,1:T(8,128)} %fusion.30, bf16[128,8,64,1]{0,2,3,1:T(8,128)(2,1)S(1)} %bitcast.82, bf16[64,128,8,64]{3,2,1,0:T(8,128)(2,1)} %reshape.303, pred[128,64,128]{0,2,1:T(8,128)(4,1)S(1)} %broadcast_compare_fusion), kind=kOutput, calls=%fused_computation.109 | convolution fusion | flops 1107230720 | bytes 76939264 | tf_op jit(solution)/shard_map/yvz,wrvz->yvwr/dot_general | solution.py:80
  309.0 16.1 %fusion.2 = (f32[128,8,64]{0,2,1:T(8,128)S(1)}, f32[128,8]{0,1:T(8,128)S(1)}) fusion(f32[128,8,64,128]{0,3,2,1:T(8,128)} %get-tuple-element.15, f32[128,8,64]{0,2,1:T(8,128)S(1)} %get-tuple-element.14, pred[128,64,128]{0,2,1:T(8,128)(4,1)S(1)} %broadcast_compare_fusion), kind=kLoop, calls=%fused_computation.8 | loop fusion | flops 33487872 | bytes 35131392 | tf_op jit(solution)/shard_map/reduce_sum | solution.py:93
  325.9 8.3 %all-to-all-start.1 = ((bf16[64,16,512]{2,1,0:T(8,128)(2,1)}), bf16[64,16,512]{2,1,0:T(8,128)(2,1)}, u32[]{:S(2)}, u32[]{:S(2)}) async-start(bf16[64,16,512]{2,1,0:T(8,128)(2,1)} %reduce-scatter.5.cloned.1.call-done), calls=%async_computation.3 | async-start | bytes 2097152 | tf_op jit(solution)/shard_map/all_to_all | solution.py:154
  334.2 20.3 %fusion.6 = f32[128,8,64]{0,2,1:T(8,128)} fusion(f32[128,8,64]{0,2,1:T(8,128)} %get-tuple-element.5, f32[128,8,64,128]{0,3,2,1:T(8,128)} %get-tuple-element.15, f32[128,8,64]{0,2,1:T(8,128)S(1)} %get-tuple-element.14, pred[128,64,128]{0,2,1:T(8,128)(4,1)S(1)} %broadcast_compare_fusion, bf16[64,128,8,64]{3,2,1,0:T(8,128)(2,1)} %reshape.304), kind=kOutput, calls=%fused_computation.12 | convolution fusion | flops 1107230720 | bytes 43778048 | tf_op jit(solution)/shard_map/qhbk,bkhd->qhbd/dot_general | solution.py:94
  357.0 5.8 %all-to-all-done.1 = bf16[64,16,512]{2,1,0:T(8,128)(2,1)} async-done(((bf16[64,16,512]{2,1,0:T(8,128)(2,1)}), bf16[64,16,512]{2,1,0:T(8,128)(2,1)}, u32[]{:S(2)}, u32[]{:S(2)}) %all-to-all-start.1) | async-done | bytes 1048608 | tf_op jit(solution)/shard_map/all_to_all | solution.py:154
  362.9 4.0 %gather_fusion.1 = bf16[512,512]{1,0:T(8,128)(2,1)} fusion(bf16[1024,512]{1,0:T(8,128)(2,1)} %bitcast.21, s32[1024]{0:T(1024)S(1)} %pad_clamp_fusion), kind=kCustom, calls=%fused_computation.1 | custom fusion | bytes 1050624 | tf_op jit(solution)/shard_map/gather | solution.py:155
  368.6 2.1 multiply_reduce_fusion
  370.6 11.7 %reduce-scatter.3.cloned.1.call-done = bf16[32,2048]{1,0:T(8,128)(2,1)} async-done(((bf16[128,2048]{1,0:T(8,128)(2,1)}), bf16[32,2048]{1,0:T(8,128)(2,1)}) %reduce-scatter.3.cloned.1.call-update) | async-done | bytes 131088 | tf_op jit(solution)/shard_map/reduce_scatter | solution.py:108
  (70 shorter events, 18.5 us)
Async XLA Ops:
  8.0 347.5 %copy-start = (bf16[512,2048]{1,0:T(8,128)(2,1)S(1)}, bf16[512,2048]{1,0:T(8,128)(2,1)}, u32[]{:S(2)}) copy-start(bf16[512,2048]{1,0:T(8,128)(2,1)} %param.26) | copy-start | bytes 6291460
  8.0 231.1 %all-gather.4.cloned.1.call-start = ((), (), s32[]{:S(2)}) async-start(), calls=%async_computation.4 | async-start | bytes 8519680 | tf_op jit(solution)/shard_map/all_gather | solution.py:70
  13.8 246.5 %all-gather.6.cloned.1.call-start = ((), (), s32[]{:S(2)}) async-start(), calls=%async_computation.5 | async-start | bytes 8519680 | tf_op jit(solution)/shard_map/all_gather | solution.py:71
  33.7 16.9 %copy-start.2 = (bf16[128,2048]{1,0:T(8,128)(2,1)S(1)}, bf16[128,2048]{1,0:T(8,128)(2,1)}, u32[]{:S(2)}) copy-start(bf16[128,2048]{1,0:T(8,128)(2,1)} %param.17) | copy-start | bytes 1572868
  33.7 16.9 %copy-start.4 = (bf16[2048,32]{0,1:T(8,128)(2,1)S(1)}, bf16[2048,32]{0,1:T(8,128)(2,1)}, u32[]{:S(2)}) copy-start(bf16[2048,32]{0,1:T(8,128)(2,1)} %param.22) | copy-start | bytes 393220
  33.7 17.0 %copy-start.5 = (f32[2048]{0:T(1024)S(1)}, f32[2048]{0:T(1024)}, u32[]{:S(2)}) copy-start(f32[2048]{0:T(1024)} %param.18) | copy-start | bytes 24580
  38.3 171.8 %all-to-all-start = ((bf16[64,16,2048]{2,1,0:T(8,128)(2,1)}), bf16[64,16,2048]{2,1,0:T(8,128)(2,1)}, u32[]{:S(2)}, u32[]{:S(2)}) async-start(bf16[64,16,2048]{2,1,0:T(8,128)(2,1)} %broadcast_select_fusion), calls=%async_computation.1 | async-start | bytes 8388608 | tf_op jit(solution)/shard_map/all_to_all | solution.py:141
  50.6 275.3 %reduce-scatter.5.cloned.1.call-start = ((), (), s32[]{:S(2)}) async-start(), calls=%async_computation.7 | async-start | bytes 5242880 | tf_op jit(solution)/shard_map/reduce_scatter | solution.py:151
  210.1 8.1 %copy-start.1 = (bf16[1,256,2048]{2,1,0:T(8,128)(2,1)S(1)}, bf16[1,256,2048]{2,1,0:T(8,128)(2,1)}, u32[]{:S(2)}) copy-start(bf16[1,256,2048]{2,1,0:T(8,128)(2,1)} %param.33) | copy-start | bytes 3145732
  325.9 37.0 %all-to-all-start.1 = ((bf16[64,16,512]{2,1,0:T(8,128)(2,1)}), bf16[64,16,512]{2,1,0:T(8,128)(2,1)}, u32[]{:S(2)}, u32[]{:S(2)}) async-start(bf16[64,16,512]{2,1,0:T(8,128)(2,1)} %reduce-scatter.5.cloned.1.call-done), calls=%async_computation.3 | async-start | bytes 2097152 | tf_op jit(solution)/shard_map/all_to_all | solution.py:154
  334.2 48.1 %reduce-scatter.3.cloned.1.call-start = ((), (), s32[]{:S(2)}) async-start(), calls=%async_computation.6 | async-start | bytes 655360 | tf_op jit(solution)/shard_map/reduce_scatter | solution.py:108
  334.2 22.6 %copy-start.3 = (f32[256,2]{0,1:T(2,128)S(1)}, f32[256,2]{0,1:T(2,128)}, u32[]{:S(2)}) copy-start(f32[256,2]{0,1:T(2,128)} %param.30) | copy-start | bytes 6148
Sparse Core Ops, SparseCore 0:
  13.9 129.2 all-gather.3
  146.6 82.3 all-gather.5
Sparse Core Ops, SparseCore 1:
  221.6 48.2 reduce-scatter.4
  356.9 25.3 reduce-scatter.2
where the time goes:
time: 392 us; the launch traced here: 390 us
  blocking collectives  155 us (40%)
  matrix products  85.8 us (22%)
  local copies, waits for them, and re-layouts  61.9 us (16%)
  other arithmetic  33 us (8%)
  starting transfers between devices  20.7 us (5%)
  waiting for transfers between devices  17.6 us (4%)
  between operations  15.8 us (4%)
    all_gather x1, blocking collectives, attention_half(): lax.all_gather(key_turned, 'ep', axis=0, tiled=True)  155 us
    dot_general x1, matrix products, attention_half(): jnp.einsum('yvz,wrvz->yvwr', query_plain, key_blocks, preferred_element_t...  27.4 us
    reshape x1, local copies, waits for them, and re-layouts, attention_half(): key_blocks = update_key_plain.reshape(blocks, row_count, head_count, NOPE)  21.2 us
    reshape x1, local copies, waits for them, and re-layouts, attention_half(): value_blocks = update_values.reshape(blocks, row_count, head_count, VD)  21.2 us
    dot_general x1, matrix products, attention_half(): jnp.einsum('qhbk,bkhd->qhbd', probs.astype(jnp.bfloat16), value_blocks, p...  20.3 us
    reduce_sum x1, other arithmetic, attention_half(): block_total = jnp.sum(probs, axis=-1)  16.1 us
    dot_general x1, matrix products, attention_half(): jnp.einsum('yjx,inx->yjin', query_rotated_rows, rotated_key_blocks, prefe...  14.9 us
    all_to_all x1, starting transfers between devices, expert_half(): lax.all_to_all(outgoing, 'ep', split_axis=0, concat_axis=0, tiled=True)  12.3 us
  transfers between devices with their start and end apart: 6, of which 2 were waited for; matrix products, arithmetic and copies ran while one was open for 45% of the time, Pallas kernels for 0%

commit v1 on v0

v1 whole, which is shorter than its diff:
```python
import functools

import jax
import jax.numpy as jnp
from jax import lax
from jax.experimental import pallas as pl
from jax.experimental.pallas import tpu as pltpu
from jax.sharding import Mesh
from jax.sharding import PartitionSpec as P


NOPE = 64
ROPE = 32
VD = 64
EPS = 1e-06
ROPE_BASE = 10000.0
F32 = jnp.float32
BF16 = jnp.bfloat16
VMEM_CAP = 60 * 1024 * 1024


def iota(shape, axis):
    return lax.broadcasted_iota(jnp.int32, shape, axis)


def dot(a, b):
    return jnp.dot(a, b, preferred_element_type=F32)


def dot_nt(a, b):
    return lax.dot_general(a, b, (((1,), (1,)), ((), ())), preferred_element_type=F32)


def params(flops=0, nbytes=0, **kw):
    return dict(
        compiler_params=pltpu.CompilerParams(vmem_limit_bytes=VMEM_CAP, **kw),
        cost_estimate=pl.CostEstimate(flops=flops, bytes_accessed=nbytes, transcendentals=0),
    )


def dispatch_kernel(t_ref, tok_ref, part_ref, gain_ref, ids_ref, *refs, capacity, experts):
    outs, tgt_ref = refs[:-1], refs[-1]
    rows = tok_ref.shape[0]
    x = tok_ref[...].astype(F32)
    inv = lax.rsqrt(jnp.mean(x * x, axis=-1, keepdims=True) + EPS)
    part = (part_ref[...].astype(F32) * inv * gain_ref[...]).astype(BF16)
    id0, id1 = ids_ref[0:1, :], ids_ref[1:2, :]
    expert = iota((experts, rows), 0)
    is0, is1 = expert == id0, expert == id1
    both = jnp.where(is0 | is1, 1.0, 0.0).astype(BF16)
    earlier = jnp.where(iota((rows, rows), 0) < iota((rows, rows), 1), 1.0, 0.0).astype(BF16)
    before = dot(both, earlier)
    slot0 = jnp.sum(jnp.where(is0, before, 0.0), axis=0, keepdims=True).astype(jnp.int32)
    slot1 = jnp.sum(jnp.where(is1, before, 0.0), axis=0, keepdims=True).astype(jnp.int32)
    chunk = capacity // len(outs)
    size = experts * chunk
    tgt0 = (slot0 // chunk) * size + id0 * chunk + slot0 % chunk
    tgt1 = (slot1 // chunk) * size + id1 * chunk + slot1 % chunk
    for c, out_ref in enumerate(outs):
        place = iota((size, rows), 0) + c * size
        sel = jnp.where((place == tgt0) | (place == tgt1), 1.0, 0.0).astype(BF16)
        out_ref[...] = dot(sel, part).astype(BF16)
    tgt_ref[...] = jnp.concatenate([tgt0, tgt1], axis=0)


def dispatch(t, tokens, gain, ids, experts, capacity, chunks, n_tp):
    rows, width = tokens.shape
    part = width // n_tp
    size = experts * capacity // chunks
    return pl.pallas_call(
        functools.partial(dispatch_kernel, capacity=capacity, experts=experts),
        grid_spec=pltpu.PrefetchScalarGridSpec(
            num_scalar_prefetch=1,
            grid=(1,),
            in_specs=[
                pl.BlockSpec((rows, width), lambda i, t: (0, 0)),
                pl.BlockSpec((rows, part), lambda i, t: (0, t[2])),
                pl.BlockSpec((1, part), lambda i, t: (0, t[2])),
                pl.BlockSpec((2, rows), lambda i, t: (0, 0)),
            ],
            out_specs=[pl.BlockSpec((size, part), lambda i, t: (0, 0))] * chunks
            + [pl.BlockSpec((2, rows), lambda i, t: (0, 0))],
        ),
        out_shape=[jax.ShapeDtypeStruct((size, part), BF16)] * chunks
        + [jax.ShapeDtypeStruct((2, rows), jnp.int32)],
        name="dispatch",
        **params(2 * rows * size * chunks * part, rows * width * 2 + size * chunks * part * 2),
    )(t, tokens, tokens, gain.reshape(1, width), ids.T)


def hidden_kernel(t_ref, x0, *refs):
    others, ws, out_ref = refs[:6], refs[6:14], refs[14]
    early = pl.program_id(0) < pl.num_programs(0) // 2
    xs = [x0[...]]
    for k in range(3):
        xs.append(jnp.where(early, others[2 * k][...], others[2 * k + 1][...]))
    gate = functools.reduce(jnp.add, [dot(x, w[...]) for x, w in zip(xs, ws[:4])])
    upp = functools.reduce(jnp.add, [dot(x, w[...]) for x, w in zip(xs, ws[4:])])
    out_ref[...] = (gate / (1.0 + jnp.exp(-gate)) * upp).astype(BF16)


def hidden_of(t, n_tp, x0, chunks, w_gate, w_up):
    rows, part = x0.shape
    width = w_gate.shape[1]
    tile = 256
    half = rows // tile // 2

    def wspec(off):
        return pl.BlockSpec((part, width), lambda i, t: (lax.rem(t[2] + off, n_tp), 0))

    row = pl.BlockSpec((tile, part), lambda i, t: (i, 0))
    first = pl.BlockSpec((tile, part), lambda i, t: (jnp.minimum(i, half - 1), 0))
    second = pl.BlockSpec((tile, part), lambda i, t: (jnp.maximum(i - half, 0), 0))
    ws = [wspec(0), wspec(n_tp - 1), wspec(1), wspec(2)]
    others = [x for pair in zip(*chunks) for x in pair]
    return pl.pallas_call(
        hidden_kernel,
        grid_spec=pltpu.PrefetchScalarGridSpec(
            num_scalar_prefetch=1,
            grid=(rows // tile,),
            in_specs=[row] + [first, second] * 3 + ws + ws,
            out_specs=pl.BlockSpec((tile, width), lambda i, t: (i, 0)),
        ),
        out_shape=jax.ShapeDtypeStruct((rows, width), BF16),
        name="hidden",
        **params(4 * rows * part * n_tp * width, rows * part * n_tp * 2),
    )(t, x0, *others, *([w_gate] * 4), *([w_up] * 4))


def columns_kernel(t_ref, w_ref, *outs):
    part = outs[0].shape[1]
    for j, out_ref in enumerate(outs):
        at = lax.rem(t_ref[2] + j, len(outs)) * part
        out_ref[...] = w_ref[:, pl.ds(pl.multiple_of(at, part), part)]


def columns_of(t, w, n_tp):
    rows, width = w.shape
    vmem = pl.BlockSpec(memory_space=pltpu.VMEM)
    return pl.pallas_call(
        columns_kernel,
        in_specs=[pl.BlockSpec(memory_space=pltpu.SMEM), vmem],
        out_specs=[vmem] * n_tp,
        out_shape=[jax.ShapeDtypeStruct((rows, width // n_tp), BF16)] * n_tp,
        name="columns",
        **params(rows * width, rows * width * 4),
    )(t, w)


def down_kernel(h0, hb, ha, fa, fb, w0, wb, wa, wf, out_ref):
    out = dot(h0[...], w0[...]) + dot(hb[...], wb[...]) + dot(ha[...], wa[...])
    half = fa.shape[0]
    out_ref[:half, :] = (out[:half] + dot(fa[...], wf[...])).astype(BF16)
    out_ref[half:, :] = (out[half:] + dot(fb[...], wf[...])).astype(BF16)


def down_of(h0, hb, ha, fa, fb, wd):
    rows, width = h0.shape
    part = wd[0].shape[1]
    return pl.pallas_call(
        down_kernel,
        out_shape=jax.ShapeDtypeStruct((rows, part), BF16),
        name="down",
        **params(2 * rows * part * len(wd) * width, rows * part * len(wd) * 2),
    )(h0, hb, ha, fa, fb, wd[0], wd[1], wd[3], wd[2])


def shares_kernel(tgt_ref, w_ref, high_ref, low_ref):
    w = w_ref[...]
    w0, w1 = w[:, 0:1], w[:, 1:2]
    total = w0 + w1
    tgt = tgt_ref[...]
    place = iota(high_ref.shape, 1)
    share = jnp.where(place == tgt[:, 0:1], w0 / total, 0.0)
    share = share + jnp.where(place == tgt[:, 1:2], w1 / total, 0.0)
    high = share.astype(BF16)
    high_ref[...] = high
    low_ref[...] = (share - high.astype(F32)).astype(BF16)


def shares_of(tgt, weights, slots):
    rows = tgt.shape[0]
    return pl.pallas_call(
        shares_kernel,
        out_shape=[jax.ShapeDtypeStruct((rows, slots), BF16)] * 2,
        name="shares",
        **params(8 * rows * slots, rows * slots * 4),
    )(tgt, weights)


def combine_kernel(ret_ref, high_ref, low_ref, out_ref):
    ret = ret_ref[...]
    out_ref[...] = (dot(high_ref[...], ret) + dot(low_ref[...], ret)).astype(BF16)


def combine(returned, high, low):
    rows = high.shape[0]
    slots, part = returned.shape
    return pl.pallas_call(
        combine_kernel,
        out_shape=jax.ShapeDtypeStruct((rows, part), BF16),
        name="combine",
        **params(4 * rows * slots * part, slots * part * 2),
    )(returned, high, low)


def project_kernel(
    tok_ref, gain_ref, wq_ref, wqr_ref, wl_ref, wkr_ref, lgain_ref, cos_ref, sin_ref, q_ref, kv_ref
):
    x = tok_ref[...].astype(F32)
    inv = lax.rsqrt(jnp.mean(x * x, axis=-1, keepdims=True) + EPS)
    normed = (x * inv * gain_ref[...]).astype(BF16)
    plain = wq_ref.shape[1]
    ranks = wl_ref.shape[1]
    cos, sin = cos_ref[...], sin_ref[...]

    def turn(v):
        n = v.shape[1]
        first = iota(v.shape, 1) % ROPE < ROPE // 2
        other = jnp.where(
            first, pltpu.roll(v, n - ROPE // 2, axis=1), pltpu.roll(v, ROPE // 2, axis=1)
        )
        return v * cos[:, :n] + other * sin[:, :n]

    q_ref[:, :plain] = dot(normed, wq_ref[...]).astype(BF16)
    q_ref[:, plain:] = turn(dot(normed, wqr_ref[...])).astype(BF16)
    raw = dot(normed, wl_ref[...])
    linv = lax.rsqrt(jnp.mean(raw * raw, axis=-1, keepdims=True) + EPS)
    kv_ref[:, :ranks] = (raw * linv * lgain_ref[...]).astype(BF16)
    key = dot_nt(normed, wkr_ref[...])
    key = jnp.concatenate([key, jnp.zeros((key.shape[0], 128 - ROPE), F32)], axis=1)
    kv_ref[:, ranks:] = turn(key).astype(BF16)


def project(tokens, gain, wq, wqr, wl, wkr, lgain, cos, sin):
    rows, width = tokens.shape
    q_width = wq.shape[1] + wqr.shape[1]
    total = q_width + wl.shape[1] + ROPE
    return pl.pallas_call(
        project_kernel,
        out_shape=[
            jax.ShapeDtypeStruct((rows, q_width), BF16),
            jax.ShapeDtypeStruct((rows, wl.shape[1] + 128), BF16),
        ],
        name="project",
        **params(2 * rows * width * total, width * total * 2),
    )(tokens, gain.reshape(1, width), wq, wqr, wl, wkr.T, lgain.reshape(1, -1), cos, sin)


def expand_kernel(wk_ref, wv_ref, *refs, heads):
    ks, (k_out, v_out) = refs[:-2], refs[-2:]
    block = ks[0].shape[0]
    ranks = wk_ref.shape[0]
    one = jnp.ones((block, 128 - VD), BF16)
    for j, k_ref in enumerate(ks):
        rows = pl.ds(j * block, block)
        lat = k_ref[:, :ranks]
        kp = dot(lat, wk_ref[...]).astype(BF16)
        vp = dot(lat, wv_ref[...]).astype(BF16)
        tail = k_ref[:, ranks:ranks + 128 - NOPE]
        for h in range(heads):
            k_out[h, rows, :] = jnp.concatenate([kp[:, h * NOPE:(h + 1) * NOPE], tail], axis=1)
            v_out[h, rows, :] = jnp.concatenate([vp[:, h * VD:(h + 1) * VD], one], axis=1)


def expand(ks, wk, wv):
    block = ks[0].shape[0]
    heads = wk.shape[1] // NOPE
    keys = block * len(ks)
    return pl.pallas_call(
        functools.partial(expand_kernel, heads=heads),
        out_shape=[jax.ShapeDtypeStruct((heads, keys, 128), BF16)] * 2,
        name="expand",
        **params(4 * keys * wk.size, keys * heads * 512),
    )(wk, wv, *ks)


def flash_kernel(at_ref, ka_ref, kb_ref, va_ref, vb_ref, *refs, heads, n_lo, n_hi, shifts):
    qs, out_ref = refs[:n_lo // 2], refs[n_lo // 2]
    q_scr, o_scr, lse_scr, bias = refs[n_lo // 2 + 1:]
    h = pl.program_id(0)
    hi, lo = at_ref[0], at_ref[1]
    block = qs[0].shape[1]
    tile = 2 * block
    n_y = n_lo // 2
    scale = (NOPE + ROPE) ** (-0.5)

    def place(i, m):
        row = lax.rem(lo // 2 - (0, 1, n_y - 1, 2)[i] + n_y, n_y)
        side = lax.rem(lo, 2)
        return row * 2 + (1 - side if m else side)

    @pl.when(h == 0)
    def _():
        lse_scr[...] = jnp.zeros_like(lse_scr)
        zero = jnp.zeros((block, 128 - NOPE - ROPE), BF16)
        gap = iota((block, block), 0) - iota((block, block), 1)
        for i in range(n_y):
            for m in range(2):
                rows = pl.ds(i * tile + m * block, block)
                for g in range(heads):
                    base = heads * NOPE + g * ROPE
                    plain = qs[i][m, :, g * NOPE:(g + 1) * NOPE]
                    turned = qs[i][m, :, base:base + ROPE]
                    q_scr[g, rows, :] = jnp.concatenate([plain, turned, zero], axis=1)
                first = hi * n_lo + place(i, m)
                for k, j in enumerate(shifts):
                    ahead = (lax.rem(hi - j + n_hi, n_hi) * n_lo + lo - first) * block
                    bias[rows, k * block:(k + 1) * block] = jnp.where(gap >= ahead, 0.0, -1e30)

    keys = jnp.concatenate([ka_ref[0], kb_ref[0]], axis=0)
    values = jnp.concatenate([va_ref[0], vb_ref[0]], axis=0)
    lane = iota((tile, 128), 1)
    for i in range(n_y):
        rows = pl.ds(i * tile, tile)
        s = dot_nt(q_scr[h, rows, :], keys) + bias[rows, :]
        top = jnp.max(s, axis=1, keepdims=True)
        p = jnp.exp2((s - top) * (scale * 1.4426950408889634)).astype(BF16)
        o = dot(p, values)
        total = o[:, VD:VD + 1]
        o_scr[h, rows, :] = (o * (1.0 / total)).astype(BF16)
        lse_scr[rows, :] = jnp.where(lane == h, top * scale + jnp.log(total), lse_scr[rows, :])

    @pl.when(h == heads - 1)
    def _():
        for i in range(n_y):
            for m in range(2):
                rows = pl.ds(i * tile + m * block, block)
                to = place(i, m)
                for g in range(heads):
                    out_ref[to, :, g * VD:(g + 1) * VD] = o_scr[g, rows, :VD]
                lse = lse_scr[rows, :]
                a = lse.astype(BF16).astype(F32)
                b = (lse - a).astype(BF16).astype(F32)
                c = lse - a - b
                packed = a + pltpu.roll(b, heads, axis=1) + pltpu.roll(c, 2 * heads, axis=1)
                out_ref[to, :, heads * VD:] = packed.astype(BF16)


def flash(at, qs, kx, vx, shifts):
    heads, keys, _ = kx[0].shape
    block = qs[0].shape[1]
    n_lo, n_hi = 2 * len(qs), len(shifts)
    rows = block * n_lo
    pair = pl.BlockSpec(qs[0].shape, lambda h, p: (0, 0, 0))
    shape = (n_lo, block, heads * VD + 128)
    return pl.pallas_call(
        functools.partial(flash_kernel, heads=heads, n_lo=n_lo, n_hi=n_hi, shifts=shifts),
        grid_spec=pltpu.PrefetchScalarGridSpec(
            num_scalar_prefetch=1,
            grid=(heads,),
            in_specs=[pl.BlockSpec((1, keys, 128), lambda h, p: (h, 0, 0))] * 4 + [pair] * len(qs),
            out_specs=pl.BlockSpec(shape, lambda h, p: (0, 0, 0)),
            scratch_shapes=[
                pltpu.VMEM((heads, rows, 128), BF16),
                pltpu.VMEM((heads, rows, 128), BF16),
                pltpu.VMEM((rows, 128), F32),
                pltpu.VMEM((rows, 2 * keys), F32),
            ],
        ),
        out_shape=jax.ShapeDtypeStruct(shape, BF16),
        name="flash",
        **params(8 * rows * keys * heads * 128, (rows * 2 + keys) * 640 * 2),
    )(at, *kx, *vx, *qs)


def merge_kernel(t_ref, parts_ref, wo_ref, *refs, heads):
    outs, scr = refs[:-1], refs[-1]
    n, rows = parts_ref.shape[:2]
    width = heads * VD
    lses = []
    for c in range(n):
        s = parts_ref[c, :, width:].astype(F32)
        lses.append(s + pltpu.roll(s, 128 - heads, axis=1) + pltpu.roll(s, 128 - 2 * heads, axis=1))
    top = functools.reduce(jnp.maximum, lses)
    factors = [jnp.exp(v - top) for v in lses]
    total = functools.reduce(jnp.add, factors)
    wide = jnp.where(iota((128, width), 1) // VD == iota((128, width), 0), 1.0, 0.0).astype(BF16)
    acc = jnp.zeros((rows, width), F32)
    for c in range(n):
        factor = factors[c] / total
        high = factor.astype(BF16)
        low = (factor - high.astype(F32)).astype(BF16)
        acc = acc + parts_ref[c, :, :width].astype(F32) * (dot(high, wide) + dot(low, wide))
    scr[...] = acc.astype(BF16)
    some = outs[0].shape[0]
    for j, out_ref in enumerate(outs):
        at = lax.rem(t_ref[2] + j, len(outs)) * some
        part = scr[pl.ds(pl.multiple_of(at, some), some), :]
        out_ref[...] = dot(part, wo_ref[...]).astype(BF16)


def merge(at, parts, wo, heads, n_tp):
    rows, width = parts.shape[1], wo.shape[1]
    vmem = pl.BlockSpec(memory_space=pltpu.VMEM)
    return pl.pallas_call(
        functools.partial(merge_kernel, heads=heads),
        in_specs=[pl.BlockSpec(memory_space=pltpu.SMEM)] + [vmem] * 2,
        out_specs=[vmem] * n_tp,
        out_shape=[jax.ShapeDtypeStruct((rows // n_tp, width), BF16)] * n_tp,
        scratch_shapes=[pltpu.VMEM((rows, heads * VD), BF16)],
        name="merge",
        **params(2 * rows * wo.shape[0] * width, wo.size * 2),
    )(at, parts, wo)


CHUNKS = 2


def round_tp(xs, n):
    up = [(i, (i + 1) % n) for i in range(n)]
    down = [(i, (i - 1) % n) for i in range(n)]
    sets = []
    for c, x in enumerate(xs):
        below = lax.ppermute(x, "tp", up)
        above = lax.ppermute(x, "tp", down)
        far = lax.ppermute(below, "tp", up) if c % 2 == 0 else lax.ppermute(above, "tp", down)
        sets.append((x, below, above, far))
    return sets


def swap_tp(xs, n):
    got = [xs[0]]
    for j in range(1, n):
        got.append(lax.ppermute(xs[j], "tp", [(i, (i + j) % n) for i in range(n)]))
    return got


def on_device(
    sizes,
    tokens_a,
    attn_gain,
    w_query,
    w_query_rot,
    w_latent,
    w_key_rot,
    latent_gain,
    w_key_up,
    w_value_up,
    w_output,
    tokens_b,
    ffn_gain,
    expert_ids,
    expert_weights,
    w_gate,
    w_up,
    w_down,
):
    n_hi, n_lo, n_tp = sizes
    n_ep = n_hi * n_lo
    hi, lo, tp = lax.axis_index("hi"), lax.axis_index("lo"), lax.axis_index("tp")
    at = jnp.stack([hi, lo, tp]).astype(jnp.int32)
    ep_axes = ("hi", "lo")

    rows_b, width = tokens_b.shape
    capacity = 2 * rows_b * expert_ids.shape[1] // n_ep
    part = width // n_tp
    outgoing, tgt = dispatch(at, tokens_b, ffn_gain, expert_ids, n_ep, capacity, 1, n_tp)
    arrived = lax.all_to_all(outgoing.reshape(n_ep, capacity, part), ep_axes, 0, 0, tiled=True)
    arrived = arrived.reshape(-1, part)

    wd = columns_of(at, w_down[0], n_tp)
    wd = swap_tp(wd, n_tp)

    rows_a = tokens_a.shape[0]
    heads = w_query.shape[1] // NOPE
    pos = ((hi * n_lo + lo) * rows_a + jnp.arange(rows_a, dtype=jnp.int32)).astype(F32)
    lane = jnp.arange(heads * ROPE, dtype=jnp.int32)
    half = ROPE // 2
    inverse = ROPE_BASE ** (-((lane % half).astype(F32) * 2.0) / ROPE)
    angles = pos[:, None] * inverse[None, :]
    cos = jnp.cos(angles)
    sin = jnp.where(lane % ROPE < half, -1.0, 1.0)[None, :] * jnp.sin(angles)
    q, kv = project(
        tokens_a, attn_gain, w_query, w_query_rot, w_latent, w_key_rot, latent_gain, cos, sin
    )

    other = [(i, i ^ 1) for i in range(n_lo)]
    up = [(i, (i + 2) % n_lo) for i in range(n_lo)]
    down = [(i, (i - 2) % n_lo) for i in range(n_lo)]
    q_other = lax.ppermute(q, "lo", other)
    pair = jnp.stack([q, q_other])
    q_below = lax.ppermute(pair, "lo", up)
    q_above = lax.ppermute(pair, "lo", down)
    q_far = lax.ppermute(q_below, "lo", up)

    def shifted(x, by):
        return lax.ppermute(x, "hi", [(i, (i + by) % n_hi) for i in range(n_hi)])

    ks = {0: kv}
    moves = ((1, 0, 1), (7, 0, -1), (2, 1, 1), (6, 7, -1), (3, 2, 1), (5, 6, -1), (4, 6, -2))
    for to, source, by in moves:
        ks[to] = shifted(ks[source], by)

    size = arrived.shape[0] // CHUNKS
    pieces = [arrived[c * size:(c + 1) * size] for c in range(CHUNKS)]
    chunks = [xs[1:] for xs in round_tp(pieces, n_tp)]
    h0 = hidden_of(at, n_tp, arrived, chunks, w_gate[0], w_up[0])
    t_up = [(i, (i + 1) % n_tp) for i in range(n_tp)]
    t_down = [(i, (i - 1) % n_tp) for i in range(n_tp)]
    hb = lax.ppermute(h0, "tp", t_up)
    ha = lax.ppermute(h0, "tp", t_down)
    fa = lax.ppermute(hb[:size], "tp", t_up)
    fb = lax.ppermute(ha[size:], "tp", t_down)
    done = down_of(h0, hb, ha, fa, fb, wd).reshape(n_ep, capacity, part)
    returned = lax.all_to_all(done, ep_axes, 0, 0, tiled=True).reshape(-1, part)
    high, low = shares_of(tgt.T, expert_weights, n_ep * capacity)
    mixed_b = combine(returned, high, low)

    near, rest = (0, 1, 7, 2), (6, 3, 5, 4)
    ka, va = expand([ks[j] for j in near], w_key_up, w_value_up)
    kb, vb = expand([ks[j] for j in rest], w_key_up, w_value_up)
    outs = flash(at, [pair, q_below, q_above, q_far], (ka, kb), (va, vb), near + rest)
    parts = lax.all_to_all(outs, "lo", 0, 0, tiled=True)
    partial = merge(at, parts, w_output, heads, n_tp)
    shared = swap_tp(partial, n_tp)
    mixed_a = functools.reduce(jnp.add, [v.astype(F32) for v in shared]).astype(BF16)
    return mixed_a, mixed_b


def solution(mesh):
    n_ep, n_tp = mesh.shape["ep"], mesh.shape["tp"]
    n_lo = 8
    n_hi = n_ep // n_lo
    grid = Mesh(mesh.devices.reshape(n_hi, n_lo, n_tp), ("hi", "lo", "tp"))
    ep = ("hi", "lo")
    placed = (
        P(ep, None),
        P(),
        P(None, "tp"),
        P(None, "tp"),
        P(),
        P(),
        P(),
        P(None, "tp"),
        P(None, "tp"),
        P("tp", None),
        P(ep, None),
        P(),
        P(ep, None),
        P(ep, None),
        P(ep, None, "tp"),
        P(ep, None, "tp"),
        P(ep, "tp", None),
    )

    def body(*args):
        return on_device((n_hi, n_lo, n_tp), *args)

    return jax.shard_map(
        body,
        mesh=grid,
        in_specs=placed,
        out_specs=(P(("hi", "lo", "tp"), None), P(ep, "tp")),
        check_vma=False,
    )
```

time: 392 us -> 205 us (0.52)
  blocking collectives: 155 us -> 0 us
  matrix products: 85.8 us -> 0 us
  Pallas kernels: 0 us -> 62.9 us
  local copies, waits for them, and re-layouts: 61.9 us -> 5.62 us
  waiting for transfers between devices: 17.6 us -> 71.2 us
  starting transfers between devices: 20.7 us -> 59 us
  other arithmetic: 33 us -> 4.41 us
  between operations: 15.8 us -> 0.98 us
    all_gather x1 -> x0, blocking collectives: 155 us -> none  [attention_half(): lax.all_gather(key_turned, 'ep', axis=0, tiled=True)]
    dot_general x13 -> x0, matrix products: 85.8 us -> none  [the longest x1 27.4 us: attention_half(): jnp.einsum('yvz,wrvz->yvwr', query_plain, key_blocks, preferred_element_t...]
    pallas_call x0 -> x11, Pallas kernels: none -> 62.9 us  [the longest x1 23 us: flash(): pl.pallas_call(functools.partial(flash_kernel, heads=heads, n_lo=n_lo, n_...]
    ppermute x0 -> x27, waiting for transfers between devices: none -> 61.5 us  [the longest x7 37.1 us: shifted(): return lax.ppermute(x, 'hi', [(i, (i + by) % n_hi) for i in range(n_hi)])]
    reshape x2 -> x0, local copies, waits for them, and re-layouts: 42.4 us -> none  [the longest x1 21.2 us: attention_half(): key_blocks = update_key_plain.reshape(blocks, row_count, head_count, NOPE)]
    ppermute x0 -> x27, starting transfers between devices: none -> 33.6 us  [the longest x6 6.98 us: swap_tp(): got.append(lax.ppermute(xs[j], 'tp', [(i, (i + j) % n) for i in range(n)]))]
    reduce_sum x7 -> x0, other arithmetic: 22 us -> none  [the longest x1 16.1 us: attention_half(): block_total = jnp.sum(probs, axis=-1)]
    reduce_scatter x2 -> x0, waiting for transfers between devices: 11.7 us -> none  [the longest x1 11.7 us: attention_half(): lax.psum_scatter(jnp.dot(attended, w_output, preferred_element_type=jnp.f...]
  transfers between devices with their start and end apart: 6 -> 30, of which waited for: 2 -> 11; matrix products, arithmetic and copies ran while one was open for 45% -> 3% of each run, Pallas kernels for 0% -> 28%
where the time goes in v1:
time: 205 us; the launch traced here: 204 us
  waiting for transfers between devices  71.2 us (35%)
  Pallas kernels  62.9 us (31%)
  starting transfers between devices  59 us (29%)
  local copies, waits for them, and re-layouts  5.62 us (3%)
  other arithmetic  4.41 us (2%)
    ppermute x7, waiting for transfers between devices, shifted(): return lax.ppermute(x, 'hi', [(i, (i + by) % n_hi) for i in range(n_hi)])  37.1 us
    pallas_call x1, Pallas kernels, flash(): pl.pallas_call(functools.partial(flash_kernel, heads=heads, n_lo=n_lo, n_...  23 us
    ppermute x6, waiting for transfers between devices, swap_tp(): got.append(lax.ppermute(xs[j], 'tp', [(i, (i + j) % n) for i in range(n)]))  12.2 us
    all_to_all x1, starting transfers between devices, on_device(): lax.all_to_all(outgoing.reshape(n_ep, capacity, part), ep_axes, 0, 0, til...  12.1 us
    all_to_all x1, waiting for transfers between devices, on_device(): returned = lax.all_to_all(done, ep_axes, 0, 0, tiled=True).reshape(-1, part)  9.64 us
    all_to_all x1, starting transfers between devices, on_device(): returned = lax.all_to_all(done, ep_axes, 0, 0, tiled=True).reshape(-1, part)  8.75 us
    ppermute x1, waiting for transfers between devices, on_device(): hb = lax.ppermute(h0, 'tp', t_up)  7.46 us
    pallas_call x1, Pallas kernels, hidden_of(): pl.pallas_call(hidden_kernel, grid_spec=pltpu.PrefetchScalarGridSpec(num_...  7.27 us
  transfers between devices with their start and end apart: 30, of which 11 were waited for; matrix products, arithmetic and copies ran while one was open for 3% of the time, Pallas kernels for 28%

profile of v1, /device:TPU:8, one launch (start us, length us, event | category | flops | bytes accessed | tf_op | source)
XLA Modules:
  0.0 204.1 jit_solution(16747187971861210969)
XLA Ops:
  1.2 3.8 %dispatch.1 = (bf16[1024,512]{1,0:T(8,128)(2,1)}, s32[2,256]{1,0:T(2,128)}) custom-call(s32[3]{0:T(128)} %pad_add_fusion.at_ref.t_ref, bf16[256,2048]{1,0:T(8,128)(2,1)} %part_ref.1, bf16[256,2048]{1,0:T(8,128)(2,1)} %part_ref.1, f32[1,2048]{1,0:T(1,128)} %bitcast.37, s32[2,256]{1,0:T(2,128)} %bitcast.40), custom_call_target="tpu_custom_call" | custom-call | flops 268435456 | bytes 2097152 | tf_op jit(solution)/shard_map/dispatch/pallas_call | solution.py:70
  4.9 12.1 %all-to-all-start.1 = ((bf16[64,16,512]{2,1,0:T(8,128)(2,1)}), bf16[64,16,512]{2,1,0:T(8,128)(2,1)S(1)}, u32[]{:S(2)}, u32[]{:S(2)}) async-start(bf16[64,16,512]{2,1,0:T(8,128)(2,1)} %bitcast.32), calls=%async_computation.1 | async-start | bytes 2097152 | tf_op jit(solution)/shard_map/all_to_all | solution.py:459
  18.3 4.9 %project.1 = (bf16[128,768]{1,0:T(8,128)(2,1)}, bf16[128,640]{1,0:T(8,128)(2,1)}) custom-call(bf16[128,2048]{1,0:T(8,128)(2,1)} %tok_ref.2, f32[1,2048]{1,0:T(1,128)} %bitcast.38, bf16[2048,512]{1,0:T(8,128)(2,1)} %wq_ref.1, bf16[2048,256]{1,0:T(8,128)(2,1)} %wqr_ref.1, bf16[2048,512]{1,0:T(8,128)(2,1)} %wl_ref.1, bf16[32,2048]{1,0:T(8,128)(2,1)} %bitcast.36, ...), custom_call_target="tpu_custom_call" | custom-call | flops 687865856 | bytes 5373952 | tf_op jit(solution)/shard_map/project/pallas_call | solution.py:239
  26.6 20.2 %collective-permute-done.refs_1_ = bf16[128,640]{1,0:T(8,128)(2,1)S(1)} collective-permute-done((bf16[128,640]{1,0:T(8,128)(2,1)}, bf16[128,640]{1,0:T(8,128)(2,1)S(1)}, u32[]{:S(2)}, u32[]{:S(2)}) %collective-permute-start) | collective-permute-done | bytes 163872 | tf_op jit(solution)/shard_map/ppermute | solution.py:488
  46.8 3.2 %collective-permute-start.3 = (bf16[128,640]{1,0:T(8,128)(2,1)S(1)}, bf16[128,640]{1,0:T(8,128)(2,1)S(1)}, u32[]{:S(2)}, u32[]{:S(2)}) collective-permute-start(bf16[128,640]{1,0:T(8,128)(2,1)S(1)} %collective-permute-done.1.refs_2_), channel_id=1, source_target_pairs={{0,224},{32,0},{64,32},{96,64},{128,96},{160,128},{192,160},{224,1... | collective-permute-start | bytes 491528 | tf_op jit(solution)/shard_map/ppermute | solution.py:488
  57.7 5.9 %collective-permute-done.4.refs_1_ = bf16[128,640]{1,0:T(8,128)(2,1)S(1)} collective-permute-done((bf16[128,640]{1,0:T(8,128)(2,1)S(1)}, bf16[128,640]{1,0:T(8,128)(2,1)S(1)}, u32[]{:S(2)}, u32[]{:S(2)}) %collective-permute-start.4) | collective-permute-done | bytes 163872 | tf_op jit(solution)/shard_map/ppermute | solution.py:488
  65.0 3.9 %collective-permute-done.5.refs_2_ = bf16[128,640]{1,0:T(8,128)(2,1)S(1)} collective-permute-done((bf16[128,640]{1,0:T(8,128)(2,1)S(1)}, bf16[128,640]{1,0:T(8,128)(2,1)S(1)}, u32[]{:S(2)}, u32[]{:S(2)}) %collective-permute-start.5) | collective-permute-done | bytes 163872 | tf_op jit(solution)/shard_map/ppermute | solution.py:488
  69.0 7.1 %collective-permute-done.6.refs_3_ = bf16[128,640]{1,0:T(8,128)(2,1)S(1)} collective-permute-done((bf16[128,640]{1,0:T(8,128)(2,1)S(1)}, bf16[128,640]{1,0:T(8,128)(2,1)S(1)}, u32[]{:S(2)}, u32[]{:S(2)}) %collective-permute-start.6) | collective-permute-done | bytes 163872 | tf_op jit(solution)/shard_map/ppermute | solution.py:488
  79.4 3.3 %collective-permute-start.19 = (bf16[512,512]{1,0:T(8,128)(2,1)S(1)}, bf16[512,512]{1,0:T(8,128)(2,1)}, u32[]{:S(2)}, u32[]{:S(2)}) collective-permute-start(bf16[512,512]{1,0:T(8,128)(2,1)S(1)} %collective-permute-done.17.refs_3_), channel_id=1, source_target_pairs={{0,3},{1,0},{2,1},{3,2},{4,7},{5,4},{6,5},{7,6},{8,11},{9,8},{10,9... | collective-permute-start | bytes 1572872 | tf_op jit(solution)/shard_map/ppermute | solution.py:417
  82.7 3.5 %expand.2 = (bf16[8,512,128]{2,1,0:T(8,128)(2,1)}, bf16[8,512,128]{2,1,0:T(8,128)(2,1)}) custom-call(bf16[512,512]{1,0:T(8,128)(2,1)} %wk_ref.3, bf16[512,512]{1,0:T(8,128)(2,1)} %wv_ref.3, bf16[128,640]{1,0:T(8,128)(2,1)} %get-tuple-element.20.refs_0_, bf16[128,640]{1,0:T(8,128)(2,1)} %copy-done.18, bf16[128,640]{1,0:T(8,128)(2,1)} %copy-done.19, ...), custom_call_target="tpu_custom_call" | custom-call | flops 536870912 | bytes 2097152 | tf_op jit(solution)/shard_map/expand/pallas_call | solution.py:270
  86.2 3.5 %expand.3 = (bf16[8,512,128]{2,1,0:T(8,128)(2,1)}, bf16[8,512,128]{2,1,0:T(8,128)(2,1)}) custom-call(bf16[512,512]{1,0:T(8,128)(2,1)} %wk_ref.3, bf16[512,512]{1,0:T(8,128)(2,1)} %wv_ref.3, bf16[128,640]{1,0:T(8,128)(2,1)} %copy-done.21, bf16[128,640]{1,0:T(8,128)(2,1)} %copy-done.22, bf16[128,640]{1,0:T(8,128)(2,1)} %copy-done.23, bf16[128,640]{1,0:T(8,128)(2,1)} %copy-done.24), custom_call_target="tpu_custom_call" | custom-call | flops 536870912 | bytes 2097152 | tf_op jit(solution)/shard_map/expand/pallas_call | solution.py:270
  89.7 23.0 %flash.1 = bf16[8,128,640]{2,1,0:T(8,128)(2,1)} custom-call(s32[3]{0:T(128)} %pad_add_fusion.at_ref.t_ref, bf16[8,512,128]{2,1,0:T(8,128)(2,1)} %get-tuple-element.21.ka_ref, bf16[8,512,128]{2,1,0:T(8,128)(2,1)} %get-tuple-element.22.kb_ref, bf16[8,512,128]{2,1,0:T(8,128)(2,1)} %get-tuple-element.23.va_ref, bf16[8,512,128]{2,1,0:T(8,128)(2,1)} %get-tuple-element.24.vb_ref, ...), custom_call_target="tpu_custom_call" | custom-call | flops 4294967296 | bytes 3276800 | tf_op jit(solution)/shard_map/flash/pallas_call | solution.py:347
  112.8 4.6 %all-to-all-start = ((bf16[8,128,640]{2,1,0:T(8,128)(2,1)}), bf16[8,128,640]{2,1,0:T(8,128)(2,1)S(1)}, u32[]{:S(2)}, u32[]{:S(2)}) async-start(bf16[8,128,640]{2,1,0:T(8,128)(2,1)} %flash.1), calls=%async_computation | async-start | bytes 2621440 | tf_op jit(solution)/shard_map/all_to_all | solution.py:514
  118.4 7.3 %hidden.1.h0 = bf16[1024,256]{1,0:T(8,128)(2,1)} custom-call(s32[3]{0:T(128)} %pad_add_fusion.at_ref.t_ref, bf16[1024,512]{1,0:T(8,128)(2,1)} %bitcast.28, bf16[512,512]{1,0:T(8,128)(2,1)} %copy-done.5, bf16[512,512]{1,0:T(8,128)(2,1)} %copy-done.7, bf16[512,512]{1,0:T(8,128)(2,1)} %copy-done.8, bf16[512,512]{1,0:T(8,128)(2,1)} %copy-done.6, ...), custom_call_target="tpu_custom_call" | custom-call | flops 2147483648 | bytes 4194304 | tf_op jit(solution)/shard_map/hidden/pallas_call | solution.py:116
  125.6 3.2 %collective-permute-start.21 = (bf16[1024,256]{1,0:T(8,128)(2,1)}, bf16[1024,256]{1,0:T(8,128)(2,1)S(1)}, u32[]{:S(2)}, u32[]{:S(2)}) collective-permute-start(bf16[1024,256]{1,0:T(8,128)(2,1)} %hidden.1.h0), channel_id=1, source_target_pairs={{0,3},{1,0},{2,1},{3,2},{4,7},{5,4},{6,5},{7,6},{8,11},{9,8},{10,9... | collective-permute-start | bytes 1572872 | tf_op jit(solution)/shard_map/ppermute | solution.py:502
  131.1 3.2 %collective-permute-start.25 = (bf16[256,512]{1,0:T(8,128)(2,1)}, bf16[256,512]{1,0:T(8,128)(2,1)S(1)}, u32[]{:S(2)}, u32[]{:S(2)}) collective-permute-start(bf16[256,512]{1,0:T(8,128)(2,1)} %get-tuple-element.33), channel_id=1, source_target_pairs={{0,3},{1,0},{2,1},{3,2},{4,7},{5,4},{6,5},{7,6},{8,11},{9,8},{10,9... | collective-permute-start | bytes 786440 | tf_op jit(solution)/shard_map/ppermute | solution.py:425
  134.4 7.5 %collective-permute-done.20.hb = bf16[1024,256]{1,0:T(8,128)(2,1)S(1)} collective-permute-done((bf16[1024,256]{1,0:T(8,128)(2,1)}, bf16[1024,256]{1,0:T(8,128)(2,1)S(1)}, u32[]{:S(2)}, u32[]{:S(2)}) %collective-permute-start.20) | collective-permute-done | bytes 524320 | tf_op jit(solution)/shard_map/ppermute | solution.py:501
  142.0 3.3 %collective-permute-start.23 = (bf16[512,256]{1,0:T(8,128)(2,1)S(1)}, bf16[512,256]{1,0:T(8,128)(2,1)S(1)}, u32[]{:S(2)}, u32[]{:S(2)}) collective-permute-start(bf16[512,256]{1,0:T(8,128)(2,1)S(1)} %slice.27), channel_id=1, source_target_pairs={{0,3},{1,0},{2,1},{3,2},{4,7},{5,4},{6,5},{7,6},{8,11},{9,8},{10,9... | collective-permute-start | bytes 786440 | tf_op jit(solution)/shard_map/ppermute | solution.py:504
  145.3 7.8 %collective-permute-done.24.wb = bf16[256,512]{1,0:T(8,128)(2,1)S(1)} collective-permute-done((bf16[256,512]{1,0:T(8,128)(2,1)}, bf16[256,512]{1,0:T(8,128)(2,1)S(1)}, u32[]{:S(2)}, u32[]{:S(2)}) %collective-permute-start.24) | collective-permute-done | bytes 262176 | tf_op jit(solution)/shard_map/ppermute | solution.py:425
  153.1 4.7 %collective-permute-done.22.fa = bf16[512,256]{1,0:T(8,128)(2,1)S(1)} collective-permute-done((bf16[512,256]{1,0:T(8,128)(2,1)S(1)}, bf16[512,256]{1,0:T(8,128)(2,1)S(1)}, u32[]{:S(2)}, u32[]{:S(2)}) %collective-permute-start.22) | collective-permute-done | bytes 262176 | tf_op jit(solution)/shard_map/ppermute | solution.py:503
  158.6 4.0 %down.1 = bf16[1024,512]{1,0:T(8,128)(2,1)} custom-call(bf16[1024,256]{1,0:T(8,128)(2,1)} %hidden.1.h0, bf16[1024,256]{1,0:T(8,128)(2,1)} %copy-done.3, bf16[1024,256]{1,0:T(8,128)(2,1)} %copy-done.4, bf16[512,256]{1,0:T(8,128)(2,1)} %copy-done.13, bf16[512,256]{1,0:T(8,128)(2,1)} %copy-done.14, bf16[256,512]{1,0:T(8,128)(2,1)} %get-tuple-element.31.w0, ...), custom_call_target="tpu_custom_call" | custom-call | flops 1073741824 | bytes 4194304 | tf_op jit(solution)/shard_map/down/pallas_call | solution.py:160
  162.7 8.8 %all-to-all-start.2 = ((bf16[64,16,512]{2,1,0:T(8,128)(2,1)}), bf16[64,16,512]{2,1,0:T(8,128)(2,1)S(1)}, u32[]{:S(2)}, u32[]{:S(2)}) async-start(bf16[64,16,512]{2,1,0:T(8,128)(2,1)} %bitcast.30), calls=%async_computation.2 | async-start | bytes 2097152 | tf_op jit(solution)/shard_map/all_to_all | solution.py:506
  171.5 5.1 %merge.1 = (bf16[32,2048]{1,0:T(8,128)(2,1)}, bf16[32,2048]{1,0:T(8,128)(2,1)}, bf16[32,2048]{1,0:T(8,128)(2,1)}, bf16[32,2048]{1,0:T(8,128)(2,1)}) custom-call(s32[3]{0:T(128)} %pad_add_fusion.at_ref.t_ref, bf16[8,128,640]{2,1,0:T(8,128)(2,1)} %copy-done.1, bf16[512,2048]{1,0:T(8,128)(2,1)} %wo_ref.1), custom_call_target="tpu_custom_call" | custom-call | flops 268435456 | bytes 2097152 | tf_op jit(solution)/shard_map/merge/pallas_call | solution.py:396
  190.6 9.6 %all-to-all-done.2 = bf16[64,16,512]{2,1,0:T(8,128)(2,1)S(1)} async-done(((bf16[64,16,512]{2,1,0:T(8,128)(2,1)}), bf16[64,16,512]{2,1,0:T(8,128)(2,1)S(1)}, u32[]{:S(2)}, u32[]{:S(2)}) %all-to-all-start.2) | async-done | bytes 1048608 | tf_op jit(solution)/shard_map/all_to_all | solution.py:506
  (108 shorter events, 39.7 us)
Async XLA Ops:
  4.9 47.6 %all-to-all-start.1 = ((bf16[64,16,512]{2,1,0:T(8,128)(2,1)}), bf16[64,16,512]{2,1,0:T(8,128)(2,1)S(1)}, u32[]{:S(2)}, u32[]{:S(2)}) async-start(bf16[64,16,512]{2,1,0:T(8,128)(2,1)} %bitcast.32), calls=%async_computation.1 | async-start | bytes 2097152 | tf_op jit(solution)/shard_map/all_to_all | solution.py:459
  23.2 26.8 %collective-permute-start.7 = (bf16[128,768]{1,0:T(8,128)(2,1)}, bf16[128,768]{1,0:T(8,128)(2,1)S(1)}, u32[]{:S(2)}, u32[]{:S(2)}) collective-permute-start(bf16[128,768]{1,0:T(8,128)(2,1)} %get-tuple-element.25), channel_id=1, source_target_pairs={{0,4},{4,0},{8,12},{12,8},{16,20},{20,16},{24,28},{28,24},{1,5},{5... | collective-permute-start | bytes 589832 | tf_op jit(solution)/shard_map/ppermute | solution.py:481
  23.3 23.5 %collective-permute-start = (bf16[128,640]{1,0:T(8,128)(2,1)}, bf16[128,640]{1,0:T(8,128)(2,1)S(1)}, u32[]{:S(2)}, u32[]{:S(2)}) collective-permute-start(bf16[128,640]{1,0:T(8,128)(2,1)} %get-tuple-element.20.refs_0_), channel_id=1, source_target_pairs={{0,32},{32,64},{64,96},{96,128},{128,160},{160,192},{192,224},{224... | collective-permute-start | bytes 491528 | tf_op jit(solution)/shard_map/ppermute | solution.py:488
  24.8 22.0 %collective-permute-start.1 = (bf16[128,640]{1,0:T(8,128)(2,1)}, bf16[128,640]{1,0:T(8,128)(2,1)S(1)}, u32[]{:S(2)}, u32[]{:S(2)}) collective-permute-start(bf16[128,640]{1,0:T(8,128)(2,1)} %get-tuple-element.20.refs_0_), channel_id=1, source_target_pairs={{0,224},{32,0},{64,32},{96,64},{128,96},{160,128},{192,160},{224,1... | collective-permute-start | bytes 491528 | tf_op jit(solution)/shard_map/ppermute | solution.py:488
  46.8 10.2 %collective-permute-start.2 = (bf16[128,640]{1,0:T(8,128)(2,1)S(1)}, bf16[128,640]{1,0:T(8,128)(2,1)S(1)}, u32[]{:S(2)}, u32[]{:S(2)}) collective-permute-start(bf16[128,640]{1,0:T(8,128)(2,1)S(1)} %collective-permute-done.refs_1_), channel_id=1, source_target_pairs={{0,32},{32,64},{64,96},{96,128},{128,160},{160,192},{192,224},{224... | collective-permute-start | bytes 491528 | tf_op jit(solution)/shard_map/ppermute | solution.py:488
  46.8 10.2 %collective-permute-start.3 = (bf16[128,640]{1,0:T(8,128)(2,1)S(1)}, bf16[128,640]{1,0:T(8,128)(2,1)S(1)}, u32[]{:S(2)}, u32[]{:S(2)}) collective-permute-start(bf16[128,640]{1,0:T(8,128)(2,1)S(1)} %collective-permute-done.1.refs_2_), channel_id=1, source_target_pairs={{0,224},{32,0},{64,32},{96,64},{128,96},{160,128},{192,160},{224,1... | collective-permute-start | bytes 491528 | tf_op jit(solution)/shard_map/ppermute | solution.py:488
  51.0 12.5 %collective-permute-start.8 = (bf16[2,128,768]{2,1,0:T(8,128)(2,1)S(1)}, bf16[2,128,768]{2,1,0:T(8,128)(2,1)}, u32[]{:S(2)}, u32[]{:S(2)}) collective-permute-start(bf16[2,128,768]{2,1,0:T(8,128)(2,1)S(1)} %pad_maximum_fusion.refs_0_), channel_id=1, source_target_pairs={{0,8},{4,12},{8,16},{12,20},{16,24},{20,28},{24,0},{28,4},{1,9},{5... | collective-permute-start | bytes 1179656 | tf_op jit(solution)/shard_map/ppermute | solution.py:483
  53.8 25.6 %collective-permute-start.14 = (bf16[512,512]{1,0:T(8,128)(2,1)}, bf16[512,512]{1,0:T(8,128)(2,1)S(1)}, u32[]{:S(2)}, u32[]{:S(2)}) collective-permute-start(bf16[512,512]{1,0:T(8,128)(2,1)} %bitcast.12), channel_id=1, source_target_pairs={{0,1},{1,2},{2,3},{3,0},{4,5},{5,6},{6,7},{7,4},{8,9},{9,10},{10,1... | collective-permute-start | bytes 1572872 | tf_op jit(solution)/shard_map/ppermute | solution.py:415
  55.3 24.1 %collective-permute-start.17 = (bf16[512,512]{1,0:T(8,128)(2,1)}, bf16[512,512]{1,0:T(8,128)(2,1)S(1)}, u32[]{:S(2)}, u32[]{:S(2)}) collective-permute-start(bf16[512,512]{1,0:T(8,128)(2,1)} %bitcast.13), channel_id=1, source_target_pairs={{0,3},{1,0},{2,1},{3,2},{4,7},{5,4},{6,5},{7,6},{8,11},{9,8},{10,9... | collective-permute-start | bytes 1572872 | tf_op jit(solution)/shard_map/ppermute | solution.py:416
  57.1 19.7 %collective-permute-start.9 = (bf16[2,128,768]{2,1,0:T(8,128)(2,1)S(1)}, bf16[2,128,768]{2,1,0:T(8,128)(2,1)S(1)}, u32[]{:S(2)}, u32[]{:S(2)}) collective-permute-start(bf16[2,128,768]{2,1,0:T(8,128)(2,1)S(1)} %pad_maximum_fusion.refs_0_), channel_id=1, source_target_pairs={{0,24},{4,28},{8,0},{12,4},{16,8},{20,12},{24,16},{28,20},{1,25},{... | collective-permute-start | bytes 1179656 | tf_op jit(solution)/shard_map/ppermute | solution.py:484
  63.6 26.2 %collective-permute-start.10 = (bf16[2,128,768]{2,1,0:T(8,128)(2,1)}, bf16[2,128,768]{2,1,0:T(8,128)(2,1)}, u32[]{:S(2)}, u32[]{:S(2)}) collective-permute-start(bf16[2,128,768]{2,1,0:T(8,128)(2,1)} %collective-permute-done.8.refs_1_), channel_id=1, source_target_pairs={{0,8},{4,12},{8,16},{12,20},{16,24},{20,28},{24,0},{28,4},{1,9},{5... | collective-permute-start | bytes 1179656 | tf_op jit(solution)/shard_map/ppermute | solution.py:485
  76.0 41.3 %collective-permute-start.15 = (bf16[512,512]{1,0:T(8,128)(2,1)}, bf16[512,512]{1,0:T(8,128)(2,1)S(1)}, u32[]{:S(2)}, u32[]{:S(2)}) collective-permute-start(bf16[512,512]{1,0:T(8,128)(2,1)} %bitcast.13), channel_id=1, source_target_pairs={{0,1},{1,2},{2,3},{3,0},{4,5},{5,6},{6,7},{7,4},{8,9},{9,10},{10,1... | collective-permute-start | bytes 1572872 | tf_op jit(solution)/shard_map/ppermute | solution.py:415
  76.8 40.6 %collective-permute-start.16 = (bf16[512,512]{1,0:T(8,128)(2,1)}, bf16[512,512]{1,0:T(8,128)(2,1)S(1)}, u32[]{:S(2)}, u32[]{:S(2)}) collective-permute-start(bf16[512,512]{1,0:T(8,128)(2,1)} %bitcast.12), channel_id=1, source_target_pairs={{0,3},{1,0},{2,1},{3,2},{4,7},{5,4},{6,5},{7,6},{8,11},{9,8},{10,9... | collective-permute-start | bytes 1572872 | tf_op jit(solution)/shard_map/ppermute | solution.py:416
  79.4 38.0 %collective-permute-start.18 = (bf16[512,512]{1,0:T(8,128)(2,1)S(1)}, bf16[512,512]{1,0:T(8,128)(2,1)}, u32[]{:S(2)}, u32[]{:S(2)}) collective-permute-start(bf16[512,512]{1,0:T(8,128)(2,1)S(1)} %collective-permute-done.14.refs_0_), channel_id=1, source_target_pairs={{0,1},{1,2},{2,3},{3,0},{4,5},{5,6},{6,7},{7,4},{8,9},{9,10},{10,1... | collective-permute-start | bytes 1572872 | tf_op jit(solution)/shard_map/ppermute | solution.py:417
  79.4 38.0 %collective-permute-start.19 = (bf16[512,512]{1,0:T(8,128)(2,1)S(1)}, bf16[512,512]{1,0:T(8,128)(2,1)}, u32[]{:S(2)}, u32[]{:S(2)}) collective-permute-start(bf16[512,512]{1,0:T(8,128)(2,1)S(1)} %collective-permute-done.17.refs_3_), channel_id=1, source_target_pairs={{0,3},{1,0},{2,1},{3,2},{4,7},{5,4},{6,5},{7,6},{8,11},{9,8},{10,9... | collective-permute-start | bytes 1572872 | tf_op jit(solution)/shard_map/ppermute | solution.py:417
  112.8 49.9 %all-to-all-start = ((bf16[8,128,640]{2,1,0:T(8,128)(2,1)}), bf16[8,128,640]{2,1,0:T(8,128)(2,1)S(1)}, u32[]{:S(2)}, u32[]{:S(2)}) async-start(bf16[8,128,640]{2,1,0:T(8,128)(2,1)} %flash.1), calls=%async_computation | async-start | bytes 2621440 | tf_op jit(solution)/shard_map/all_to_all | solution.py:514
  125.6 16.2 %collective-permute-start.20 = (bf16[1024,256]{1,0:T(8,128)(2,1)}, bf16[1024,256]{1,0:T(8,128)(2,1)S(1)}, u32[]{:S(2)}, u32[]{:S(2)}) collective-permute-start(bf16[1024,256]{1,0:T(8,128)(2,1)} %hidden.1.h0), channel_id=1, source_target_pairs={{0,1},{1,2},{2,3},{3,0},{4,5},{5,6},{6,7},{7,4},{8,9},{9,10},{10,1... | collective-permute-start | bytes 1572872 | tf_op jit(solution)/shard_map/ppermute | solution.py:501
  125.6 16.3 %collective-permute-start.21 = (bf16[1024,256]{1,0:T(8,128)(2,1)}, bf16[1024,256]{1,0:T(8,128)(2,1)S(1)}, u32[]{:S(2)}, u32[]{:S(2)}) collective-permute-start(bf16[1024,256]{1,0:T(8,128)(2,1)} %hidden.1.h0), channel_id=1, source_target_pairs={{0,3},{1,0},{2,1},{3,2},{4,7},{5,4},{6,5},{7,6},{8,11},{9,8},{10,9... | collective-permute-start | bytes 1572872 | tf_op jit(solution)/shard_map/ppermute | solution.py:502
  131.1 21.9 %collective-permute-start.24 = (bf16[256,512]{1,0:T(8,128)(2,1)}, bf16[256,512]{1,0:T(8,128)(2,1)S(1)}, u32[]{:S(2)}, u32[]{:S(2)}) collective-permute-start(bf16[256,512]{1,0:T(8,128)(2,1)} %get-tuple-element.32), channel_id=1, source_target_pairs={{0,1},{1,2},{2,3},{3,0},{4,5},{5,6},{6,7},{7,4},{8,9},{9,10},{10,1... | collective-permute-start | bytes 786440 | tf_op jit(solution)/shard_map/ppermute | solution.py:425
  131.1 21.9 %collective-permute-start.25 = (bf16[256,512]{1,0:T(8,128)(2,1)}, bf16[256,512]{1,0:T(8,128)(2,1)S(1)}, u32[]{:S(2)}, u32[]{:S(2)}) collective-permute-start(bf16[256,512]{1,0:T(8,128)(2,1)} %get-tuple-element.33), channel_id=1, source_target_pairs={{0,3},{1,0},{2,1},{3,2},{4,7},{5,4},{6,5},{7,6},{8,11},{9,8},{10,9... | collective-permute-start | bytes 786440 | tf_op jit(solution)/shard_map/ppermute | solution.py:425
  134.4 18.7 %collective-permute-start.26 = (bf16[256,512]{1,0:T(8,128)(2,1)}, bf16[256,512]{1,0:T(8,128)(2,1)S(1)}, u32[]{:S(2)}, u32[]{:S(2)}) collective-permute-start(bf16[256,512]{1,0:T(8,128)(2,1)} %get-tuple-element.34), channel_id=1, source_target_pairs={{0,2},{1,3},{2,0},{3,1},{4,6},{5,7},{6,4},{7,5},{8,10},{9,11},{10,... | collective-permute-start | bytes 786440 | tf_op jit(solution)/shard_map/ppermute | solution.py:425
  141.9 16.0 %collective-permute-start.22 = (bf16[512,256]{1,0:T(8,128)(2,1)S(1)}, bf16[512,256]{1,0:T(8,128)(2,1)S(1)}, u32[]{:S(2)}, u32[]{:S(2)}) collective-permute-start(bf16[512,256]{1,0:T(8,128)(2,1)S(1)} %slice.26), channel_id=1, source_target_pairs={{0,1},{1,2},{2,3},{3,0},{4,5},{5,6},{6,7},{7,4},{8,9},{9,10},{10,1... | collective-permute-start | bytes 786440 | tf_op jit(solution)/shard_map/ppermute | solution.py:503
  142.0 15.8 %collective-permute-start.23 = (bf16[512,256]{1,0:T(8,128)(2,1)S(1)}, bf16[512,256]{1,0:T(8,128)(2,1)S(1)}, u32[]{:S(2)}, u32[]{:S(2)}) collective-permute-start(bf16[512,256]{1,0:T(8,128)(2,1)S(1)} %slice.27), channel_id=1, source_target_pairs={{0,3},{1,0},{2,1},{3,2},{4,7},{5,4},{6,5},{7,6},{8,11},{9,8},{10,9... | collective-permute-start | bytes 786440 | tf_op jit(solution)/shard_map/ppermute | solution.py:504
  162.7 37.5 %all-to-all-start.2 = ((bf16[64,16,512]{2,1,0:T(8,128)(2,1)}), bf16[64,16,512]{2,1,0:T(8,128)(2,1)S(1)}, u32[]{:S(2)}, u32[]{:S(2)}) async-start(bf16[64,16,512]{2,1,0:T(8,128)(2,1)} %bitcast.30), calls=%async_computation.2 | async-start | bytes 2097152 | tf_op jit(solution)/shard_map/all_to_all | solution.py:506
  (31 other events, 385.3 us)

commit v2 on v1

--- a/solution.py
+++ b/solution.py
@@ -17,6 +17,7 @@
 F32 = jnp.float32
 BF16 = jnp.bfloat16
 VMEM_CAP = 60 * 1024 * 1024
+VMEM_ALL = 67043328
 
 
 def iota(shape, axis):
@@ -31,9 +32,9 @@
     return lax.dot_general(a, b, (((1,), (1,)), ((), ())), preferred_element_type=F32)
 
 
-def params(flops=0, nbytes=0, **kw):
+def params(flops=0, nbytes=0, cap=VMEM_CAP):
     return dict(
-        compiler_params=pltpu.CompilerParams(vmem_limit_bytes=VMEM_CAP, **kw),
+        compiler_params=pltpu.CompilerParams(vmem_limit_bytes=cap),
         cost_estimate=pl.CostEstimate(flops=flops, bytes_accessed=nbytes, transcendentals=0),
     )
 
@@ -196,11 +197,16 @@
 def combine(returned, high, low):
     rows = high.shape[0]
     slots, part = returned.shape
+    tile = 256
+    share = pl.BlockSpec((rows, slots), lambda i: (0, 0))
     return pl.pallas_call(
         combine_kernel,
+        grid=(part // tile,),
+        in_specs=[pl.BlockSpec((slots, tile), lambda i: (0, i)), share, share],
+        out_specs=pl.BlockSpec((rows, tile), lambda i: (0, i)),
         out_shape=jax.ShapeDtypeStruct((rows, part), BF16),
         name="combine",
-        **params(4 * rows * slots * part, slots * part * 2),
+        **params(4 * rows * slots * part, slots * part * 2, cap=VMEM_ALL),
     )(returned, high, low)
 
 
@@ -259,8 +265,10 @@
         vp = dot(lat, wv_ref[...]).astype(BF16)
         tail = k_ref[:, ranks:ranks + 128 - NOPE]
         for h in range(heads):
-            k_out[h, rows, :] = jnp.concatenate([kp[:, h * NOPE:(h + 1) * NOPE], tail], axis=1)
-            v_out[h, rows, :] = jnp.concatenate([vp[:, h * VD:(h + 1) * VD], one], axis=1)
+            k_out[h, rows, :NOPE] = kp[:, h * NOPE:(h + 1) * NOPE]
+            k_out[h, rows, NOPE:] = tail
+            v_out[h, rows, :VD] = vp[:, h * VD:(h + 1) * VD]
+            v_out[h, rows, VD:] = one
 
 
 def expand(ks, wk, wv):

time: 205 us -> 205 us (level)
  no operation moved by 1% of the time
where the time goes in v2:
time: 205 us; the launch traced here: 204 us
  waiting for transfers between devices  71 us (35%)
  Pallas kernels  63.3 us (31%)
  starting transfers between devices  59.2 us (29%)
  local copies, waits for them, and re-layouts  4.64 us (2%)
  other arithmetic  4.5 us (2%)
    ppermute x7, waiting for transfers between devices, shifted(): return lax.ppermute(x, 'hi', [(i, (i + by) % n_hi) for i in range(n_hi)])  37.1 us
    pallas_call x1, Pallas kernels, flash(): pl.pallas_call(functools.partial(flash_kernel, heads=heads, n_lo=n_lo, n_...  23 us
    ppermute x6, waiting for transfers between devices, swap_tp(): got.append(lax.ppermute(xs[j], 'tp', [(i, (i + j) % n) for i in range(n)]))  12.1 us
    all_to_all x1, starting transfers between devices, on_device(): lax.all_to_all(outgoing.reshape(n_ep, capacity, part), ep_axes, 0, 0, til...  12.1 us
    all_to_all x1, waiting for transfers between devices, on_device(): returned = lax.all_to_all(done, ep_axes, 0, 0, tiled=True).reshape(-1, part)  9.55 us
    all_to_all x1, starting transfers between devices, on_device(): returned = lax.all_to_all(done, ep_axes, 0, 0, tiled=True).reshape(-1, part)  8.93 us
    ppermute x1, waiting for transfers between devices, on_device(): hb = lax.ppermute(h0, 'tp', t_up)  7.45 us
    pallas_call x2, Pallas kernels, expand(): pl.pallas_call(functools.partial(expand_kernel, heads=heads), out_shape=[...  7.35 us
  transfers between devices with their start and end apart: 30, of which 11 were waited for; matrix products, arithmetic and copies ran while one was open for 3% of the time, Pallas kernels for 28%

profile of v2, /device:TPU:8, one launch (start us, length us, event | category | flops | bytes accessed | tf_op | source)
XLA Modules:
  0.0 203.6 jit_solution(5666049967589875656)
XLA Ops:
  1.3 3.8 %dispatch.1 = (bf16[1024,512]{1,0:T(8,128)(2,1)}, s32[2,256]{1,0:T(2,128)}) custom-call(s32[3]{0:T(128)} %pad_add_fusion.at_ref.t_ref, bf16[256,2048]{1,0:T(8,128)(2,1)} %part_ref.1, bf16[256,2048]{1,0:T(8,128)(2,1)} %part_ref.1, f32[1,2048]{1,0:T(1,128)} %bitcast.36, s32[2,256]{1,0:T(2,128)} %bitcast.39), custom_call_target="tpu_custom_call" | custom-call | flops 268435456 | bytes 2097152 | tf_op jit(solution)/shard_map/dispatch/pallas_call | solution.py:71
  5.0 12.1 %all-to-all-start.1 = ((bf16[64,16,512]{2,1,0:T(8,128)(2,1)}), bf16[64,16,512]{2,1,0:T(8,128)(2,1)S(1)}, u32[]{:S(2)}, u32[]{:S(2)}) async-start(bf16[64,16,512]{2,1,0:T(8,128)(2,1)} %bitcast.31), calls=%async_computation.1 | async-start | bytes 2097152 | tf_op jit(solution)/shard_map/all_to_all | solution.py:467
  18.4 4.9 %project.1 = (bf16[128,768]{1,0:T(8,128)(2,1)}, bf16[128,640]{1,0:T(8,128)(2,1)}) custom-call(bf16[128,2048]{1,0:T(8,128)(2,1)} %tok_ref.2, f32[1,2048]{1,0:T(1,128)} %bitcast.37, bf16[2048,512]{1,0:T(8,128)(2,1)} %wq_ref.1, bf16[2048,256]{1,0:T(8,128)(2,1)} %wqr_ref.1, bf16[2048,512]{1,0:T(8,128)(2,1)} %wl_ref.1, bf16[32,2048]{1,0:T(8,128)(2,1)} %bitcast.35, ...), custom_call_target="tpu_custom_call" | custom-call | flops 687865856 | bytes 5373952 | tf_op jit(solution)/shard_map/project/pallas_call | solution.py:245
  26.7 20.2 %collective-permute-done.refs_1_ = bf16[128,640]{1,0:T(8,128)(2,1)S(1)} collective-permute-done((bf16[128,640]{1,0:T(8,128)(2,1)}, bf16[128,640]{1,0:T(8,128)(2,1)S(1)}, u32[]{:S(2)}, u32[]{:S(2)}) %collective-permute-start) | collective-permute-done | bytes 163872 | tf_op jit(solution)/shard_map/ppermute | solution.py:496
  46.9 3.2 %collective-permute-start.3 = (bf16[128,640]{1,0:T(8,128)(2,1)S(1)}, bf16[128,640]{1,0:T(8,128)(2,1)S(1)}, u32[]{:S(2)}, u32[]{:S(2)}) collective-permute-start(bf16[128,640]{1,0:T(8,128)(2,1)S(1)} %collective-permute-done.1.refs_2_), channel_id=1, source_target_pairs={{0,224},{32,0},{64,32},{96,64},{128,96},{160,128},{192,160},{224,1... | collective-permute-start | bytes 491528 | tf_op jit(solution)/shard_map/ppermute | solution.py:496
  57.8 5.9 %collective-permute-done.4.refs_1_ = bf16[128,640]{1,0:T(8,128)(2,1)S(1)} collective-permute-done((bf16[128,640]{1,0:T(8,128)(2,1)S(1)}, bf16[128,640]{1,0:T(8,128)(2,1)S(1)}, u32[]{:S(2)}, u32[]{:S(2)}) %collective-permute-start.4) | collective-permute-done | bytes 163872 | tf_op jit(solution)/shard_map/ppermute | solution.py:496
  65.1 3.9 %collective-permute-done.5.refs_2_ = bf16[128,640]{1,0:T(8,128)(2,1)S(1)} collective-permute-done((bf16[128,640]{1,0:T(8,128)(2,1)S(1)}, bf16[128,640]{1,0:T(8,128)(2,1)S(1)}, u32[]{:S(2)}, u32[]{:S(2)}) %collective-permute-start.5) | collective-permute-done | bytes 163872 | tf_op jit(solution)/shard_map/ppermute | solution.py:496
  69.0 7.1 %collective-permute-done.6.refs_3_ = bf16[128,640]{1,0:T(8,128)(2,1)S(1)} collective-permute-done((bf16[128,640]{1,0:T(8,128)(2,1)S(1)}, bf16[128,640]{1,0:T(8,128)(2,1)S(1)}, u32[]{:S(2)}, u32[]{:S(2)}) %collective-permute-start.6) | collective-permute-done | bytes 163872 | tf_op jit(solution)/shard_map/ppermute | solution.py:496
  79.5 3.3 %collective-permute-start.19 = (bf16[512,512]{1,0:T(8,128)(2,1)S(1)}, bf16[512,512]{1,0:T(8,128)(2,1)}, u32[]{:S(2)}, u32[]{:S(2)}) collective-permute-start(bf16[512,512]{1,0:T(8,128)(2,1)S(1)} %collective-permute-done.17.refs_3_), channel_id=1, source_target_pairs={{0,3},{1,0},{2,1},{3,2},{4,7},{5,4},{6,5},{7,6},{8,11},{9,8},{10,9... | collective-permute-start | bytes 1572872 | tf_op jit(solution)/shard_map/ppermute | solution.py:425
  82.8 3.7 %expand.2 = (bf16[8,512,128]{2,1,0:T(8,128)(2,1)}, bf16[8,512,128]{2,1,0:T(8,128)(2,1)}) custom-call(bf16[512,512]{1,0:T(8,128)(2,1)} %wk_ref.3, bf16[512,512]{1,0:T(8,128)(2,1)} %wv_ref.3, bf16[128,640]{1,0:T(8,128)(2,1)} %get-tuple-element.20.refs_0_, bf16[128,640]{1,0:T(8,128)(2,1)} %copy-done.17, bf16[128,640]{1,0:T(8,128)(2,1)} %copy-done.18, ...), custom_call_target="tpu_custom_call" | custom-call | flops 536870912 | bytes 2097152 | tf_op jit(solution)/shard_map/expand/pallas_call | solution.py:278
  86.5 3.7 %expand.3 = (bf16[8,512,128]{2,1,0:T(8,128)(2,1)}, bf16[8,512,128]{2,1,0:T(8,128)(2,1)}) custom-call(bf16[512,512]{1,0:T(8,128)(2,1)} %wk_ref.3, bf16[512,512]{1,0:T(8,128)(2,1)} %wv_ref.3, bf16[128,640]{1,0:T(8,128)(2,1)} %copy-done.20, bf16[128,640]{1,0:T(8,128)(2,1)} %copy-done.21, bf16[128,640]{1,0:T(8,128)(2,1)} %copy-done.22, bf16[128,640]{1,0:T(8,128)(2,1)} %copy-done.23), custom_call_target="tpu_custom_call" | custom-call | flops 536870912 | bytes 2097152 | tf_op jit(solution)/shard_map/expand/pallas_call | solution.py:278
  90.2 23.0 %flash.1 = bf16[8,128,640]{2,1,0:T(8,128)(2,1)} custom-call(s32[3]{0:T(128)} %pad_add_fusion.at_ref.t_ref, bf16[8,512,128]{2,1,0:T(8,128)(2,1)} %get-tuple-element.21.ka_ref, bf16[8,512,128]{2,1,0:T(8,128)(2,1)} %get-tuple-element.22.kb_ref, bf16[8,512,128]{2,1,0:T(8,128)(2,1)} %get-tuple-element.23.va_ref, bf16[8,512,128]{2,1,0:T(8,128)(2,1)} %get-tuple-element.24.vb_ref, ...), custom_call_target="tpu_custom_call" | custom-call | flops 4294967296 | bytes 3276800 | tf_op jit(solution)/shard_map/flash/pallas_call | solution.py:355
  113.2 4.5 %all-to-all-start = ((bf16[8,128,640]{2,1,0:T(8,128)(2,1)}), bf16[8,128,640]{2,1,0:T(8,128)(2,1)S(1)}, u32[]{:S(2)}, u32[]{:S(2)}) async-start(bf16[8,128,640]{2,1,0:T(8,128)(2,1)} %flash.1), calls=%async_computation | async-start | bytes 2621440 | tf_op jit(solution)/shard_map/all_to_all | solution.py:522
  118.7 7.3 %hidden.1.h0 = bf16[1024,256]{1,0:T(8,128)(2,1)} custom-call(s32[3]{0:T(128)} %pad_add_fusion.at_ref.t_ref, bf16[1024,512]{1,0:T(8,128)(2,1)} %bitcast.28, bf16[512,512]{1,0:T(8,128)(2,1)} %copy-done.4, bf16[512,512]{1,0:T(8,128)(2,1)} %copy-done.6, bf16[512,512]{1,0:T(8,128)(2,1)} %copy-done.7, bf16[512,512]{1,0:T(8,128)(2,1)} %copy-done.5, ...), custom_call_target="tpu_custom_call" | custom-call | flops 2147483648 | bytes 4194304 | tf_op jit(solution)/shard_map/hidden/pallas_call | solution.py:117
  126.0 3.2 %collective-permute-start.21 = (bf16[1024,256]{1,0:T(8,128)(2,1)}, bf16[1024,256]{1,0:T(8,128)(2,1)S(1)}, u32[]{:S(2)}, u32[]{:S(2)}) collective-permute-start(bf16[1024,256]{1,0:T(8,128)(2,1)} %hidden.1.h0), channel_id=1, source_target_pairs={{0,3},{1,0},{2,1},{3,2},{4,7},{5,4},{6,5},{7,6},{8,11},{9,8},{10,9... | collective-permute-start | bytes 1572872 | tf_op jit(solution)/shard_map/ppermute | solution.py:510
  131.5 3.2 %collective-permute-start.25 = (bf16[256,512]{1,0:T(8,128)(2,1)}, bf16[256,512]{1,0:T(8,128)(2,1)S(1)}, u32[]{:S(2)}, u32[]{:S(2)}) collective-permute-start(bf16[256,512]{1,0:T(8,128)(2,1)} %get-tuple-element.33), channel_id=1, source_target_pairs={{0,3},{1,0},{2,1},{3,2},{4,7},{5,4},{6,5},{7,6},{8,11},{9,8},{10,9... | collective-permute-start | bytes 786440 | tf_op jit(solution)/shard_map/ppermute | solution.py:433
  134.8 7.5 %collective-permute-done.20.hb = bf16[1024,256]{1,0:T(8,128)(2,1)S(1)} collective-permute-done((bf16[1024,256]{1,0:T(8,128)(2,1)}, bf16[1024,256]{1,0:T(8,128)(2,1)S(1)}, u32[]{:S(2)}, u32[]{:S(2)}) %collective-permute-start.20) | collective-permute-done | bytes 524320 | tf_op jit(solution)/shard_map/ppermute | solution.py:509
  142.4 3.3 %collective-permute-start.23 = (bf16[512,256]{1,0:T(8,128)(2,1)S(1)}, bf16[512,256]{1,0:T(8,128)(2,1)S(1)}, u32[]{:S(2)}, u32[]{:S(2)}) collective-permute-start(bf16[512,256]{1,0:T(8,128)(2,1)S(1)} %slice.27), channel_id=1, source_target_pairs={{0,3},{1,0},{2,1},{3,2},{4,7},{5,4},{6,5},{7,6},{8,11},{9,8},{10,9... | collective-permute-start | bytes 786440 | tf_op jit(solution)/shard_map/ppermute | solution.py:512
  145.7 7.8 %collective-permute-done.24.wb = bf16[256,512]{1,0:T(8,128)(2,1)S(1)} collective-permute-done((bf16[256,512]{1,0:T(8,128)(2,1)}, bf16[256,512]{1,0:T(8,128)(2,1)S(1)}, u32[]{:S(2)}, u32[]{:S(2)}) %collective-permute-start.24) | collective-permute-done | bytes 262176 | tf_op jit(solution)/shard_map/ppermute | solution.py:433
  153.5 4.7 %collective-permute-done.22.fa = bf16[512,256]{1,0:T(8,128)(2,1)S(1)} collective-permute-done((bf16[512,256]{1,0:T(8,128)(2,1)S(1)}, bf16[512,256]{1,0:T(8,128)(2,1)S(1)}, u32[]{:S(2)}, u32[]{:S(2)}) %collective-permute-start.22) | collective-permute-done | bytes 262176 | tf_op jit(solution)/shard_map/ppermute | solution.py:511
  159.0 4.0 %down.1 = bf16[1024,512]{1,0:T(8,128)(2,1)} custom-call(bf16[1024,256]{1,0:T(8,128)(2,1)} %hidden.1.h0, bf16[1024,256]{1,0:T(8,128)(2,1)} %copy-done.2, bf16[1024,256]{1,0:T(8,128)(2,1)} %copy-done.3, bf16[512,256]{1,0:T(8,128)(2,1)} %copy-done.12, bf16[512,256]{1,0:T(8,128)(2,1)} %copy-done.13, bf16[256,512]{1,0:T(8,128)(2,1)} %get-tuple-element.31.w0, ...), custom_call_target="tpu_custom_call" | custom-call | flops 1073741824 | bytes 4194304 | tf_op jit(solution)/shard_map/down/pallas_call | solution.py:161
  163.1 8.9 %all-to-all-start.2 = ((bf16[64,16,512]{2,1,0:T(8,128)(2,1)}), bf16[64,16,512]{2,1,0:T(8,128)(2,1)}, u32[]{:S(2)}, u32[]{:S(2)}) async-start(bf16[64,16,512]{2,1,0:T(8,128)(2,1)} %bitcast.29), calls=%async_computation.2 | async-start | bytes 2097152 | tf_op jit(solution)/shard_map/all_to_all | solution.py:514
  172.0 5.1 %merge.1 = (bf16[32,2048]{1,0:T(8,128)(2,1)}, bf16[32,2048]{1,0:T(8,128)(2,1)}, bf16[32,2048]{1,0:T(8,128)(2,1)}, bf16[32,2048]{1,0:T(8,128)(2,1)}) custom-call(s32[3]{0:T(128)} %pad_add_fusion.at_ref.t_ref, bf16[8,128,640]{2,1,0:T(8,128)(2,1)} %copy-done.1, bf16[512,2048]{1,0:T(8,128)(2,1)} %wo_ref.1), custom_call_target="tpu_custom_call" | custom-call | flops 268435456 | bytes 2097152 | tf_op jit(solution)/shard_map/merge/pallas_call | solution.py:404
  191.1 9.6 %all-to-all-done.2 = bf16[64,16,512]{2,1,0:T(8,128)(2,1)} async-done(((bf16[64,16,512]{2,1,0:T(8,128)(2,1)}), bf16[64,16,512]{2,1,0:T(8,128)(2,1)}, u32[]{:S(2)}, u32[]{:S(2)}) %all-to-all-start.2) | async-done | bytes 1048608 | tf_op jit(solution)/shard_map/all_to_all | solution.py:514
  (106 shorter events, 38.8 us)
Async XLA Ops:
  5.0 47.6 %all-to-all-start.1 = ((bf16[64,16,512]{2,1,0:T(8,128)(2,1)}), bf16[64,16,512]{2,1,0:T(8,128)(2,1)S(1)}, u32[]{:S(2)}, u32[]{:S(2)}) async-start(bf16[64,16,512]{2,1,0:T(8,128)(2,1)} %bitcast.31), calls=%async_computation.1 | async-start | bytes 2097152 | tf_op jit(solution)/shard_map/all_to_all | solution.py:467
  23.3 26.8 %collective-permute-start.7 = (bf16[128,768]{1,0:T(8,128)(2,1)}, bf16[128,768]{1,0:T(8,128)(2,1)S(1)}, u32[]{:S(2)}, u32[]{:S(2)}) collective-permute-start(bf16[128,768]{1,0:T(8,128)(2,1)} %get-tuple-element.25), channel_id=1, source_target_pairs={{0,4},{4,0},{8,12},{12,8},{16,20},{20,16},{24,28},{28,24},{1,5},{5... | collective-permute-start | bytes 589832 | tf_op jit(solution)/shard_map/ppermute | solution.py:489
  23.5 23.4 %collective-permute-start = (bf16[128,640]{1,0:T(8,128)(2,1)}, bf16[128,640]{1,0:T(8,128)(2,1)S(1)}, u32[]{:S(2)}, u32[]{:S(2)}) collective-permute-start(bf16[128,640]{1,0:T(8,128)(2,1)} %get-tuple-element.20.refs_0_), channel_id=1, source_target_pairs={{0,32},{32,64},{64,96},{96,128},{128,160},{160,192},{192,224},{224... | collective-permute-start | bytes 491528 | tf_op jit(solution)/shard_map/ppermute | solution.py:496
  24.9 22.0 %collective-permute-start.1 = (bf16[128,640]{1,0:T(8,128)(2,1)}, bf16[128,640]{1,0:T(8,128)(2,1)S(1)}, u32[]{:S(2)}, u32[]{:S(2)}) collective-permute-start(bf16[128,640]{1,0:T(8,128)(2,1)} %get-tuple-element.20.refs_0_), channel_id=1, source_target_pairs={{0,224},{32,0},{64,32},{96,64},{128,96},{160,128},{192,160},{224,1... | collective-permute-start | bytes 491528 | tf_op jit(solution)/shard_map/ppermute | solution.py:496
  46.9 10.2 %collective-permute-start.2 = (bf16[128,640]{1,0:T(8,128)(2,1)S(1)}, bf16[128,640]{1,0:T(8,128)(2,1)S(1)}, u32[]{:S(2)}, u32[]{:S(2)}) collective-permute-start(bf16[128,640]{1,0:T(8,128)(2,1)S(1)} %collective-permute-done.refs_1_), channel_id=1, source_target_pairs={{0,32},{32,64},{64,96},{96,128},{128,160},{160,192},{192,224},{224... | collective-permute-start | bytes 491528 | tf_op jit(solution)/shard_map/ppermute | solution.py:496
  46.9 10.2 %collective-permute-start.3 = (bf16[128,640]{1,0:T(8,128)(2,1)S(1)}, bf16[128,640]{1,0:T(8,128)(2,1)S(1)}, u32[]{:S(2)}, u32[]{:S(2)}) collective-permute-start(bf16[128,640]{1,0:T(8,128)(2,1)S(1)} %collective-permute-done.1.refs_2_), channel_id=1, source_target_pairs={{0,224},{32,0},{64,32},{96,64},{128,96},{160,128},{192,160},{224,1... | collective-permute-start | bytes 491528 | tf_op jit(solution)/shard_map/ppermute | solution.py:496
  51.1 12.5 %collective-permute-start.8 = (bf16[2,128,768]{2,1,0:T(8,128)(2,1)S(1)}, bf16[2,128,768]{2,1,0:T(8,128)(2,1)}, u32[]{:S(2)}, u32[]{:S(2)}) collective-permute-start(bf16[2,128,768]{2,1,0:T(8,128)(2,1)S(1)} %pad_maximum_fusion.refs_0_), channel_id=1, source_target_pairs={{0,8},{4,12},{8,16},{12,20},{16,24},{20,28},{24,0},{28,4},{1,9},{5... | collective-permute-start | bytes 1179656 | tf_op jit(solution)/shard_map/ppermute | solution.py:491
  53.9 25.6 %collective-permute-start.14 = (bf16[512,512]{1,0:T(8,128)(2,1)}, bf16[512,512]{1,0:T(8,128)(2,1)S(1)}, u32[]{:S(2)}, u32[]{:S(2)}) collective-permute-start(bf16[512,512]{1,0:T(8,128)(2,1)} %bitcast.12), channel_id=1, source_target_pairs={{0,1},{1,2},{2,3},{3,0},{4,5},{5,6},{6,7},{7,4},{8,9},{9,10},{10,1... | collective-permute-start | bytes 1572872 | tf_op jit(solution)/shard_map/ppermute | solution.py:423
  55.4 24.1 %collective-permute-start.17 = (bf16[512,512]{1,0:T(8,128)(2,1)}, bf16[512,512]{1,0:T(8,128)(2,1)S(1)}, u32[]{:S(2)}, u32[]{:S(2)}) collective-permute-start(bf16[512,512]{1,0:T(8,128)(2,1)} %bitcast.13), channel_id=1, source_target_pairs={{0,3},{1,0},{2,1},{3,2},{4,7},{5,4},{6,5},{7,6},{8,11},{9,8},{10,9... | collective-permute-start | bytes 1572872 | tf_op jit(solution)/shard_map/ppermute | solution.py:424
  57.1 19.7 %collective-permute-start.9 = (bf16[2,128,768]{2,1,0:T(8,128)(2,1)S(1)}, bf16[2,128,768]{2,1,0:T(8,128)(2,1)S(1)}, u32[]{:S(2)}, u32[]{:S(2)}) collective-permute-start(bf16[2,128,768]{2,1,0:T(8,128)(2,1)S(1)} %pad_maximum_fusion.refs_0_), channel_id=1, source_target_pairs={{0,24},{4,28},{8,0},{12,4},{16,8},{20,12},{24,16},{28,20},{1,25},{... | collective-permute-start | bytes 1179656 | tf_op jit(solution)/shard_map/ppermute | solution.py:492
  63.7 26.5 %collective-permute-start.10 = (bf16[2,128,768]{2,1,0:T(8,128)(2,1)}, bf16[2,128,768]{2,1,0:T(8,128)(2,1)}, u32[]{:S(2)}, u32[]{:S(2)}) collective-permute-start(bf16[2,128,768]{2,1,0:T(8,128)(2,1)} %collective-permute-done.8.refs_1_), channel_id=1, source_target_pairs={{0,8},{4,12},{8,16},{12,20},{16,24},{20,28},{24,0},{28,4},{1,9},{5... | collective-permute-start | bytes 1179656 | tf_op jit(solution)/shard_map/ppermute | solution.py:493
  76.1 41.6 %collective-permute-start.15 = (bf16[512,512]{1,0:T(8,128)(2,1)}, bf16[512,512]{1,0:T(8,128)(2,1)S(1)}, u32[]{:S(2)}, u32[]{:S(2)}) collective-permute-start(bf16[512,512]{1,0:T(8,128)(2,1)} %bitcast.13), channel_id=1, source_target_pairs={{0,1},{1,2},{2,3},{3,0},{4,5},{5,6},{6,7},{7,4},{8,9},{9,10},{10,1... | collective-permute-start | bytes 1572872 | tf_op jit(solution)/shard_map/ppermute | solution.py:423
  76.9 40.8 %collective-permute-start.16 = (bf16[512,512]{1,0:T(8,128)(2,1)}, bf16[512,512]{1,0:T(8,128)(2,1)S(1)}, u32[]{:S(2)}, u32[]{:S(2)}) collective-permute-start(bf16[512,512]{1,0:T(8,128)(2,1)} %bitcast.12), channel_id=1, source_target_pairs={{0,3},{1,0},{2,1},{3,2},{4,7},{5,4},{6,5},{7,6},{8,11},{9,8},{10,9... | collective-permute-start | bytes 1572872 | tf_op jit(solution)/shard_map/ppermute | solution.py:424
  79.5 38.3 %collective-permute-start.18 = (bf16[512,512]{1,0:T(8,128)(2,1)S(1)}, bf16[512,512]{1,0:T(8,128)(2,1)}, u32[]{:S(2)}, u32[]{:S(2)}) collective-permute-start(bf16[512,512]{1,0:T(8,128)(2,1)S(1)} %collective-permute-done.14.refs_0_), channel_id=1, source_target_pairs={{0,1},{1,2},{2,3},{3,0},{4,5},{5,6},{6,7},{7,4},{8,9},{9,10},{10,1... | collective-permute-start | bytes 1572872 | tf_op jit(solution)/shard_map/ppermute | solution.py:425
  79.5 38.3 %collective-permute-start.19 = (bf16[512,512]{1,0:T(8,128)(2,1)S(1)}, bf16[512,512]{1,0:T(8,128)(2,1)}, u32[]{:S(2)}, u32[]{:S(2)}) collective-permute-start(bf16[512,512]{1,0:T(8,128)(2,1)S(1)} %collective-permute-done.17.refs_3_), channel_id=1, source_target_pairs={{0,3},{1,0},{2,1},{3,2},{4,7},{5,4},{6,5},{7,6},{8,11},{9,8},{10,9... | collective-permute-start | bytes 1572872 | tf_op jit(solution)/shard_map/ppermute | solution.py:425
  113.2 49.9 %all-to-all-start = ((bf16[8,128,640]{2,1,0:T(8,128)(2,1)}), bf16[8,128,640]{2,1,0:T(8,128)(2,1)S(1)}, u32[]{:S(2)}, u32[]{:S(2)}) async-start(bf16[8,128,640]{2,1,0:T(8,128)(2,1)} %flash.1), calls=%async_computation | async-start | bytes 2621440 | tf_op jit(solution)/shard_map/all_to_all | solution.py:522
  126.0 16.2 %collective-permute-start.20 = (bf16[1024,256]{1,0:T(8,128)(2,1)}, bf16[1024,256]{1,0:T(8,128)(2,1)S(1)}, u32[]{:S(2)}, u32[]{:S(2)}) collective-permute-start(bf16[1024,256]{1,0:T(8,128)(2,1)} %hidden.1.h0), channel_id=1, source_target_pairs={{0,1},{1,2},{2,3},{3,0},{4,5},{5,6},{6,7},{7,4},{8,9},{9,10},{10,1... | collective-permute-start | bytes 1572872 | tf_op jit(solution)/shard_map/ppermute | solution.py:509
  126.0 16.3 %collective-permute-start.21 = (bf16[1024,256]{1,0:T(8,128)(2,1)}, bf16[1024,256]{1,0:T(8,128)(2,1)S(1)}, u32[]{:S(2)}, u32[]{:S(2)}) collective-permute-start(bf16[1024,256]{1,0:T(8,128)(2,1)} %hidden.1.h0), channel_id=1, source_target_pairs={{0,3},{1,0},{2,1},{3,2},{4,7},{5,4},{6,5},{7,6},{8,11},{9,8},{10,9... | collective-permute-start | bytes 1572872 | tf_op jit(solution)/shard_map/ppermute | solution.py:510
  131.5 21.9 %collective-permute-start.24 = (bf16[256,512]{1,0:T(8,128)(2,1)}, bf16[256,512]{1,0:T(8,128)(2,1)S(1)}, u32[]{:S(2)}, u32[]{:S(2)}) collective-permute-start(bf16[256,512]{1,0:T(8,128)(2,1)} %get-tuple-element.32), channel_id=1, source_target_pairs={{0,1},{1,2},{2,3},{3,0},{4,5},{5,6},{6,7},{7,4},{8,9},{9,10},{10,1... | collective-permute-start | bytes 786440 | tf_op jit(solution)/shard_map/ppermute | solution.py:433
  131.5 21.9 %collective-permute-start.25 = (bf16[256,512]{1,0:T(8,128)(2,1)}, bf16[256,512]{1,0:T(8,128)(2,1)S(1)}, u32[]{:S(2)}, u32[]{:S(2)}) collective-permute-start(bf16[256,512]{1,0:T(8,128)(2,1)} %get-tuple-element.33), channel_id=1, source_target_pairs={{0,3},{1,0},{2,1},{3,2},{4,7},{5,4},{6,5},{7,6},{8,11},{9,8},{10,9... | collective-permute-start | bytes 786440 | tf_op jit(solution)/shard_map/ppermute | solution.py:433
  134.8 18.7 %collective-permute-start.26 = (bf16[256,512]{1,0:T(8,128)(2,1)}, bf16[256,512]{1,0:T(8,128)(2,1)S(1)}, u32[]{:S(2)}, u32[]{:S(2)}) collective-permute-start(bf16[256,512]{1,0:T(8,128)(2,1)} %get-tuple-element.34), channel_id=1, source_target_pairs={{0,2},{1,3},{2,0},{3,1},{4,6},{5,7},{6,4},{7,5},{8,10},{9,11},{10,... | collective-permute-start | bytes 786440 | tf_op jit(solution)/shard_map/ppermute | solution.py:433
  142.3 16.0 %collective-permute-start.22 = (bf16[512,256]{1,0:T(8,128)(2,1)S(1)}, bf16[512,256]{1,0:T(8,128)(2,1)S(1)}, u32[]{:S(2)}, u32[]{:S(2)}) collective-permute-start(bf16[512,256]{1,0:T(8,128)(2,1)S(1)} %slice.26), channel_id=1, source_target_pairs={{0,1},{1,2},{2,3},{3,0},{4,5},{5,6},{6,7},{7,4},{8,9},{9,10},{10,1... | collective-permute-start | bytes 786440 | tf_op jit(solution)/shard_map/ppermute | solution.py:511
  142.4 15.8 %collective-permute-start.23 = (bf16[512,256]{1,0:T(8,128)(2,1)S(1)}, bf16[512,256]{1,0:T(8,128)(2,1)S(1)}, u32[]{:S(2)}, u32[]{:S(2)}) collective-permute-start(bf16[512,256]{1,0:T(8,128)(2,1)S(1)} %slice.27), channel_id=1, source_target_pairs={{0,3},{1,0},{2,1},{3,2},{4,7},{5,4},{6,5},{7,6},{8,11},{9,8},{10,9... | collective-permute-start | bytes 786440 | tf_op jit(solution)/shard_map/ppermute | solution.py:512
  163.1 37.6 %all-to-all-start.2 = ((bf16[64,16,512]{2,1,0:T(8,128)(2,1)}), bf16[64,16,512]{2,1,0:T(8,128)(2,1)}, u32[]{:S(2)}, u32[]{:S(2)}) async-start(bf16[64,16,512]{2,1,0:T(8,128)(2,1)} %bitcast.29), calls=%async_computation.2 | async-start | bytes 2097152 | tf_op jit(solution)/shard_map/all_to_all | solution.py:514
  (30 other events, 386.2 us)
